TPU v7x, 32 devices: a whole 2x2x4 slice. The times are simulated.
32 devices in a mesh: sp: 8 (over z, y), tp: 4 (over x, core).
Axes of the slice: x: 2, y: 2, z: 4, core: 2. Of those that a mesh axis runs over, the one named last changes fastest.
Arguments:
- layer_grad: bfloat16 [1536, 2048], P('sp'), may hold values from -6 to 6
- routes: int32 [1536, 2], P('sp'), may hold values from 0 to 7, as said below
- route_weight: float32 [1536, 2], P('sp'), may hold values from 0.1 to 0.9
- slot_tokens: bfloat16 [8, 576, 2048], P('sp'), may hold values from -6 to 6
- gate_proj: bfloat16 [8, 2048, 1024], P('sp', None, 'tp'), may hold values from -0.125 to 0.125
- up_proj: bfloat16 [8, 2048, 1024], P('sp', None, 'tp'), may hold values from -0.125 to 0.125
- down_proj: bfloat16 [8, 1024, 2048], P('sp', 'tp'), may hold values from -0.1875 to 0.1875
- out_proj: bfloat16 [2048, 1024], P(None, 'tp'), may hold values from -0.1875 to 0.1875
- queries: bfloat16 [1536, 512], P('sp', 'tp'), may hold values from -6 to 6
- keys: bfloat16 [1536, 512], P('sp', 'tp'), may hold values from -6 to 6
- values: bfloat16 [1536, 1024], P('sp', 'tp'), may hold values from -6 to 6
- fwd_decay: float32 [1536, 512], P('sp', 'tp'), may hold values from -2 to 0
- bwd_decay: float32 [1536, 512], P('sp', 'tp'), may hold values from -2 to 0
Outputs:
- gate_grad: bfloat16 [8, 2048, 1024], P('sp', None, 'tp')
- up_grad: bfloat16 [8, 2048, 1024], P('sp', None, 'tp')
- down_grad: bfloat16 [8, 1024, 2048], P('sp', 'tp')
- proj_grad: float32 [2048, 1024], P('sp', 'tp')
- query_grad: bfloat16 [1536, 512], P('sp', 'tp')
- key_grad: bfloat16 [1536, 512], P('sp', 'tp')
- value_grad: bfloat16 [1536, 1024], P('sp', 'tp')
Inputs may be any that keep to these rules, and one draw needn't show every extreme that they name: `routes`: each row names two different experts of one group of 8 consecutive experts. In every aligned block of 192 rows one expert is named by 72 rows or more.
All inputs are finite; a program needn't handle non-finite values.
Results may differ from a plain program's by a relative error of at most 0.015.
Values may be sent and summed in bfloat16 or wider, within the bound.
A program may use at most 128 MiB of HBM per device.

v0:
```python
import jax
import jax.numpy as jnp
from jax import lax
from jax.sharding import PartitionSpec as P

KEY_CHANNELS = 64
DV = 128
BLOCK = 64


EPSILON = 1e-06


def carried_in(part, axis, combine, identity, reverse):
    count = lax.axis_size(axis)
    place = lax.axis_index(axis)
    ahead = count - 1 - place if reverse else place
    gathered = jax.tree.map(lambda a: lax.all_gather(a, axis), part)
    state = jax.tree.map(lambda a, e: jnp.zeros_like(a) + jnp.asarray(e, a.dtype), part, identity)

    def one(hop, state):
        source = count - 1 - hop if reverse else hop
        return combine(
            state, jax.tree.map(lambda a: lax.dynamic_index_in_dim(a, source, 0, False), gathered)
        )

    return lax.fori_loop(0, ahead, one, state)


def sweep(query_rows, keyrows, valrows, log_decay, strict):
    nheads, length, kwidth = query_rows.shape
    vwidth = valrows.shape[-1]
    number = length // BLOCK
    offset = -1 if strict else 0
    causal = jnp.tril(jnp.ones((BLOCK, BLOCK), jnp.float32), offset)

    def split(array):
        return jnp.moveaxis(array.reshape(nheads, number, BLOCK, array.shape[-1]), 1, 0)

    def advance(carried_state, pieces):
        query_block, key_block, value_block, gblock = pieces
        running_total = jnp.cumsum(gblock, axis=1)
        middle = running_total[:, BLOCK // 2 - 1 : BLOCK // 2, :]
        scores = (
            jnp.einsum(
                "hik,hjk->hij",
                query_block * jnp.exp(running_total - middle),
                key_block * jnp.exp(middle - running_total),
                precision=lax.Precision.HIGHEST,
            )
            * causal
        )
        inner = jnp.einsum("hij,hjv->hiv", scores, value_block, precision=lax.Precision.HIGHEST)
        outer_product = jnp.einsum(
            "zuw,zwo->zuo",
            query_block * jnp.exp(running_total),
            carried_state,
            precision=lax.Precision.HIGHEST,
        )
        final_row = running_total[:, -1:, :]
        fresh_state = jnp.einsum(
            "xor,xot->xrt",
            key_block * jnp.exp(final_row - running_total),
            value_block,
            precision=lax.Precision.HIGHEST,
        )
        return (
            jnp.exp(final_row[:, 0, :])[:, :, None] * carried_state + fresh_state,
            inner + outer_product,
        )

    start_state = jnp.zeros((nheads, kwidth, vwidth), jnp.float32)
    final, outputs = lax.scan(
        advance, start_state, (split(query_rows), split(keyrows), split(valrows), split(log_decay))
    )
    return (jnp.moveaxis(outputs, 0, 1).reshape(nheads, length, vwidth), final)


def slot_ranks(expert_ids, experts):
    members = (expert_ids[:, None] == jnp.arange(experts, dtype=jnp.int32)[None, :]).astype(
        jnp.int32
    )
    before = jnp.cumsum(members, axis=0) - members
    return jnp.sum(before * members, axis=1)


def local_pass(query_rows, keyrows, valrows, fwd_log, bwd_log):
    forward_out, forward_end = sweep(query_rows, keyrows, valrows, fwd_log, False)
    backward_out, backward_end = sweep(
        jnp.flip(query_rows, 1),
        jnp.flip(keyrows, 1),
        jnp.flip(valrows, 1),
        jnp.flip(bwd_log, 1),
        True,
    )
    return (forward_out, forward_end, jnp.flip(backward_out, 1), backward_end)


def finish(query_rows, fwd_log, bwd_log, forward_out, backward_out, forward_entry, backward_entry):
    rising_decay = jnp.exp(jnp.cumsum(fwd_log, axis=1))
    falling_decay = jnp.exp(jnp.flip(jnp.cumsum(jnp.flip(bwd_log, 1), axis=1), 1))
    mixed = forward_out + backward_out
    mixed = mixed + jnp.einsum(
        "xfj,xji->xfi", query_rows * rising_decay, forward_entry, precision=lax.Precision.HIGHEST
    )
    mixed = mixed + jnp.einsum(
        "xfj,xji->xfi", query_rows * falling_decay, backward_entry, precision=lax.Precision.HIGHEST
    )
    return mixed * lax.rsqrt(jnp.mean(mixed * mixed, axis=-1, keepdims=True) + EPSILON)


def combine(earlier, later):
    return (earlier[0] * later[0], later[0][:, :, None] * earlier[1] + later[1])


def carry(decays, terms, backward):
    identity = (jnp.ones_like(decays), jnp.zeros_like(terms))
    return carried_in((decays, terms), "sp", combine, identity, backward)[1]


def on_device(
    layer_grad,
    routes,
    route_weight,
    slot_tokens,
    gate_proj,
    up_proj,
    down_proj,
    out_proj,
    queries,
    keys,
    values,
    fwd_decay,
    bwd_decay,
):
    devices = lax.axis_size("sp")
    rows_here = layer_grad.shape[0]
    width = layer_grad.shape[1]
    slots = slot_tokens.shape[1]
    capacity = slots // devices
    expert_ids = routes.reshape(-1)
    ranks = slot_ranks(expert_ids, devices)
    kept = ranks < capacity
    target = jnp.where(kept, expert_ids * capacity + ranks, slots)
    sender = (
        jnp.full((slots + 1,), -1, jnp.int32)
        .at[target]
        .set(jnp.arange(2 * rows_here, dtype=jnp.int32))[:slots]
    )
    anchor = jnp.maximum(sender, 0)
    scaled = route_weight.reshape(-1)[anchor] * (sender >= 0).astype(jnp.float32)
    column_share = width // lax.axis_size("tp")
    own_slice = lax.dynamic_slice_in_dim(
        layer_grad, lax.axis_index("tp") * column_share, column_share, 1
    )
    outgoing = (own_slice[anchor // 2].astype(jnp.float32) * scaled[:, None]).astype(jnp.bfloat16)
    arrived = lax.all_to_all(
        outgoing.reshape(devices, capacity, column_share),
        "sp",
        split_axis=0,
        concat_axis=0,
        tiled=True,
    ).reshape(slots, column_share)
    inbound = lax.all_gather(arrived, "tp", axis=1, tiled=True)
    inputs = slot_tokens[0]
    w_gate = gate_proj[0]
    w_upper = up_proj[0]
    w_down = down_proj[0]
    gate = jnp.dot(inputs, w_gate, preferred_element_type=jnp.float32)
    upper = jnp.dot(inputs, w_upper, preferred_element_type=jnp.float32)
    sigma = jax.nn.sigmoid(gate)
    act = (gate * sigma * upper).astype(jnp.bfloat16)
    grad_down = lax.dot_general(
        act, inbound, (((0,), (0,)), ((), ())), preferred_element_type=jnp.float32
    )
    act_grad = lax.dot_general(
        inbound, w_down, (((1,), (1,)), ((), ())), preferred_element_type=jnp.float32
    )
    up_delta = (act_grad * gate * sigma).astype(jnp.bfloat16)
    gate_delta = (act_grad * upper * sigma * (1.0 + gate * (1.0 - sigma))).astype(jnp.bfloat16)
    grad_gate = lax.dot_general(
        inputs, gate_delta, (((0,), (0,)), ((), ())), preferred_element_type=jnp.float32
    )
    grad_up = lax.dot_general(
        inputs, up_delta, (((0,), (0,)), ((), ())), preferred_element_type=jnp.float32
    )
    slot_part = lax.dot_general(
        gate_delta, w_gate, (((1,), (1,)), ((), ())), preferred_element_type=jnp.float32
    )
    slot_part = slot_part + lax.dot_general(
        up_delta, w_upper, (((1,), (1,)), ((), ())), preferred_element_type=jnp.float32
    )
    safe_target = jnp.minimum(target, slots - 1)
    kept_float = kept.astype(jnp.float32)[:, None]
    summed = lax.psum(slot_part.astype(jnp.bfloat16), "tp")
    backrows = lax.all_to_all(
        summed.reshape(devices, capacity, width), "sp", split_axis=0, concat_axis=0, tiled=True
    ).reshape(slots, width)
    picked = backrows[safe_target].astype(jnp.float32) * kept_float
    moe_grad = jnp.sum(picked.reshape(rows_here, 2, width), axis=1)
    stream_grad = (layer_grad.astype(jnp.float32) + moe_grad).astype(jnp.bfloat16)
    scale = KEY_CHANNELS ** (-0.5)

    def split_heads(array, size):
        return array.astype(jnp.float32).reshape(rows_here, -1, size).transpose(1, 0, 2)

    def merge_heads(array):
        return array.transpose(1, 0, 2).reshape(rows_here, -1)

    query_heads = split_heads(queries, KEY_CHANNELS) * scale
    fwd_heads = split_heads(fwd_decay, KEY_CHANNELS)
    bwd_heads = split_heads(bwd_decay, KEY_CHANNELS)
    local_out, local_pull = jax.vjp(
        local_pass,
        query_heads,
        split_heads(keys, KEY_CHANNELS),
        split_heads(values, DV),
        fwd_heads,
        bwd_heads,
    )
    forward_out, forward_end, backward_out, backward_end = local_out
    fwd_total = jnp.exp(jnp.sum(fwd_heads, axis=1))
    bwd_total = jnp.exp(jnp.sum(bwd_heads, axis=1))
    forward_entry = carry(fwd_total, forward_end, False)
    backward_entry = carry(bwd_total, backward_end, True)
    mixed, finish_pull = jax.vjp(
        finish,
        query_heads,
        fwd_heads,
        bwd_heads,
        forward_out,
        backward_out,
        forward_entry,
        backward_entry,
    )
    mixed_rows = merge_heads(mixed).astype(jnp.bfloat16)
    proj_grad = lax.psum_scatter(
        lax.dot_general(
            stream_grad, mixed_rows, (((0,), (0,)), ((), ())), preferred_element_type=jnp.float32
        ),
        "sp",
        scatter_dimension=0,
        tiled=True,
    )
    mixed_grad = jnp.dot(stream_grad, out_proj, preferred_element_type=jnp.float32)
    query_first, fwd_first, bwd_first, forward_cot, backward_cot, fwd_direct, bwd_direct = (
        finish_pull(split_heads(mixed_grad, DV))
    )
    fwd_after = carry(fwd_total, fwd_direct, True)
    bwd_after = carry(bwd_total, bwd_direct, False)
    query_second, key_part, value_part, fwd_unused, bwd_unused = local_pull(
        (forward_cot, fwd_after, backward_cot, bwd_after)
    )
    query_grad = (merge_heads(query_first + query_second) * scale).astype(jnp.bfloat16)
    return (
        grad_gate.astype(jnp.bfloat16)[None],
        grad_up.astype(jnp.bfloat16)[None],
        grad_down.astype(jnp.bfloat16)[None],
        proj_grad,
        query_grad,
        merge_heads(key_part).astype(jnp.bfloat16),
        merge_heads(value_part).astype(jnp.bfloat16),
    )


def solution(mesh):
    placed = (
        P("sp", None),
        P("sp", None),
        P("sp", None),
        P("sp", None, None),
        P("sp", None, "tp"),
        P("sp", None, "tp"),
        P("sp", "tp", None),
        P(None, "tp"),
        P("sp", "tp"),
        P("sp", "tp"),
        P("sp", "tp"),
        P("sp", "tp"),
        P("sp", "tp"),
    )
    return jax.shard_map(
        on_device,
        mesh=mesh,
        in_specs=placed,
        out_specs=(
            P("sp", None, "tp"),
            P("sp", None, "tp"),
            P("sp", "tp", None),
            P("sp", "tp"),
            P("sp", "tp"),
            P("sp", "tp"),
            P("sp", "tp"),
        ),
        check_vma=False,
    )
```

profile of v0, /device:TPU:0, one launch (start us, length us, event | category | flops | bytes accessed | tf_op | source)
XLA Modules:
  0.0 467.0 jit_solution(18426476392055585856)
XLA Ops:
  11.2 2.9 scatter_custom_fusion
  15.1 4.0 gather_fusion.1
  20.1 2.7 gather_fusion
  23.9 7.4 %all-to-all-start = ((bf16[8,72,512]{2,1,0:T(8,128)(2,1)}), bf16[8,72,512]{2,1,0:T(8,128)(2,1)}, u32[]{:S(2)}, u32[]{:S(2)}) async-start(bf16[8,72,512]{2,1,0:T(8,128)(2,1)} %fusion.179), calls=%async_computation | async-start | bytes 1179648 | tf_op jit(solution)/shard_map/all_to_all | solution.py:157
  45.0 14.3 %while.171 = (s32[]{:T(128)}, f32[2,64,128]{2,1,0:T(8,128)S(1)}, f32[3,2,64,128]{3,2,1,0:T(8,128)}, f32[3,2,64,64]{3,2,1,0:T(8,128)}, f32[3,2,64,64]{3,2,1,0:T(8...) while((s32[]{:T(128)}, f32[2,64,128]{2,1,0:T(8,128)S(1)}, ...), condition=%wide.region_11.12_spmd.clone, body=%wide.region_9.11_spmd.clone.sunk | while | flops 44785664 | bytes 2162159 | solution.py:73
  67.1 2.4 reduce-window.24
  69.5 3.3 reduce-window.26
  74.2 2.9 fusion.175
  86.4 18.2 %while.170 = (s32[]{:T(128)}, f32[2,64,128]{2,1,0:T(8,128)S(1)}, f32[3,2,64,128]{3,2,1,0:T(8,128)}, f32[3,2,64,64]{3,2,1,0:T(8,128)}, f32[3,2,64,64]{3,2,1,0:T(8...) while((s32[]{:T(128)}, f32[2,64,128]{2,1,0:T(8,128)S(1)}, ...), condition=%wide.region_8.9_spmd.clone, body=%wide.region_6.8_spmd.clone.sunk | while | flops 44785664 | bytes 2161895 | solution.py:73
  104.6 3.3 multiply_convert_fusion.1
  109.3 2.2 add_convert_fusion
  112.7 33.8 %all-gather.1 = f32[16,64,128]{2,1,0:T(8,128)} all-gather(f32[2,64,128]{2,1,0:T(8,128)S(1)} %get-tuple-element.1225), channel_id=3, replica_groups=mesh['sp'=8,'tp'=4] {'sp'}, dimensions={0}, use_global_device_ids=true | all-gather | bytes 589824 | tf_op jit(solution)/shard_map/all_gather | solution.py:18
  146.5 34.3 %all-gather.3 = f32[16,64,128]{2,1,0:T(8,128)} all-gather(f32[2,64,128]{2,1,0:T(8,128)S(1)} %get-tuple-element.1227), channel_id=5, replica_groups=mesh['sp'=8,'tp'=4] {'sp'}, dimensions={0}, use_global_device_ids=true | all-gather | bytes 589824 | tf_op jit(solution)/shard_map/all_gather | solution.py:18
  182.6 8.8 %all-to-all-start.1 = ((bf16[8,72,2048]{2,1,0:T(8,128)(2,1)}), bf16[8,72,2048]{2,1,0:T(8,128)(2,1)}, u32[]{:S(2)}, u32[]{:S(2)}) async-start(bf16[8,72,2048]{2,1,0:T(8,128)(2,1)} %all-reduce.4.cloned.1.call-done), calls=%async_computation.1 | async-start | bytes 4718592 | tf_op jit(solution)/shard_map/all_to_all | solution.py:196
  192.9 2.9 rev.39
  197.6 32.4 %all-gather.6 = f32[8,2,64]{2,1,0:T(2,128)S(1)} all-gather(f32[1,2,64]{2,1,0:T(2,128)S(1)} %copy-done.30), channel_id=2, replica_groups=mesh['sp'=8,'tp'=4] {'sp'}, dimensions={0}, use_global_device_ids=true | all-gather | bytes 4608 | tf_op jit(solution)/shard_map/all_gather | solution.py:18
  229.9 26.0 %all-gather.7 = f32[8,2,64]{2,1,0:T(2,128)S(1)} all-gather(f32[1,2,64]{2,1,0:T(2,128)S(1)} %copy-done.31), channel_id=4, replica_groups=mesh['sp'=8,'tp'=4] {'sp'}, dimensions={0}, use_global_device_ids=true | all-gather | bytes 4608 | tf_op jit(solution)/shard_map/all_gather | solution.py:18
  256.0 1.7 bitcast_add_fusion.6
  257.7 2.2 convolution_add_fusion.9
  259.9 6.8 %while.165 = (s32[]{:T(128)}, f32[2,64,128]{2,1,0:T(8,128)S(1)}, s32[]{:T(128)}, f32[8,2,64]{2,1,0:T(2,128)S(1)}, f32[8,2,64,128]{3,2,1,0:T(8,128)}, /*index=5*/s32[]{:T(128)}, s32[]{:T(128)}, s32[]{:T(128)}, s32[]{:T(128)}) while((s32[]{:T(128)}, f32[2,64,128]{2,1,0:T(8,128)S(1)}, s32[]{:T(128)}, f32[8,2,64]{2,1,0:T(2,128)S(1)}, ...), condition=%wide.region_21.22_spmd, body=%wide.region_20.21_spmd.sunk | while | flops 32774 | bytes 198299 | solution.py:27
  266.7 2.0 fusion.170
  268.7 2.3 copy.209
  271.0 2.9 fusion.171
  273.9 2.3 copy.210
  276.1 4.0 fusion.172
  280.2 7.0 %gather_fusion.2 = bf16[384,2048]{1,0:T(8,128)(2,1)} fusion(bf16[576,2048]{1,0:T(8,128)(2,1)} %bitcast.22, s32[1024]{0:T(1024)S(1)} %pad_clamp_fusion), kind=kCustom, calls=%fused_computation.2 | custom fusion | bytes 3147264 | tf_op jit(solution)/shard_map/gather | solution.py:199
  287.2 4.8 %reshape.470 = f32[192,2,2048]{2,1,0:T(2,128)} reshape(bf16[384,2048]{1,0:T(8,128)(2,1)} %gather_fusion.2) | data formatting | bytes 4718592 | tf_op jit(solution)/shard_map/convert_element_type | solution.py:199
  292.0 7.0 %multiply_reduce_fusion = f32[192,2048]{1,0:T(8,128)S(1)} fusion(f32[192,2,2048]{2,1,0:T(2,128)} %reshape.470, f32[192,2]{1,0:T(8,128)S(1)} %copy-done.21), kind=kLoop, calls=%fused_computation.243 | loop fusion | flops 1179648 | bytes 4720128 | tf_op jit(solution)/shard_map/reduce_sum | solution.py:200
  304.5 3.5 fusion.199
  308.0 33.9 %all-gather.5 = f32[16,64,128]{2,1,0:T(8,128)} all-gather(f32[2,64,128]{2,1,0:T(8,128)S(1)} %copy-done.23), channel_id=7, replica_groups=mesh['sp'=8,'tp'=4] {'sp'}, dimensions={0}, use_global_device_ids=true | all-gather | bytes 589824 | tf_op jit(solution)/shard_map/all_gather | solution.py:18
  342.0 6.9 %while.167 = (s32[]{:T(128)}, f32[2,64,128]{2,1,0:T(8,128)S(1)}, s32[]{:T(128)}, f32[8,2,64]{2,1,0:T(2,128)S(1)}, f32[8,2,64,128]{3,2,1,0:T(8,128)}, /*index=5*/s32[]{:T(128)}, s32[]{:T(128)}, s32[]{:T(128)}, s32[]{:T(128)}) while((s32[]{:T(128)}, f32[2,64,128]{2,1,0:T(8,128)S(1)}, s32[]{:T(128)}, f32[8,2,64]{2,1,0:T(2,128)S(1)}, ...), condition=%wide.region_30.31_spmd, body=%wide.region_29.30_spmd.sunk | while | flops 32774 | bytes 198299 | solution.py:27
  348.9 33.8 %all-gather.4 = f32[16,64,128]{2,1,0:T(8,128)} all-gather(f32[2,64,128]{2,1,0:T(8,128)S(1)} %copy-done.22), channel_id=6, replica_groups=mesh['sp'=8,'tp'=4] {'sp'}, dimensions={0}, use_global_device_ids=true | all-gather | bytes 589824 | tf_op jit(solution)/shard_map/all_gather | solution.py:18
  385.7 29.8 %while.168 = (s32[]{:T(128)}, f32[2,64,128]{2,1,0:T(8,128)S(1)}, f32[3,2,64,64]{3,2,1,0:T(8,128)}, f32[3,2,64,64]{3,2,1,0:T(8,128)}, f32[3,2,64,128]{3,2,0,1:T(8...) while((s32[]{:T(128)}, f32[2,64,128]{2,1,0:T(8,128)S(1)}, ...), condition=%wide.region_28.29_spmd.clone, body=%wide.region_27.28_spmd.clone.sunk | while | flops 88195072 | bytes 1894873 | solution.py:73
  392.1 1.8 fusion.318
  393.9 1.8 fusion.320
  400.4 1.7 fusion.317
  402.1 1.8 fusion.318
  403.8 1.7 fusion.320
  412.0 1.8 fusion.318
  413.8 1.7 fusion.320
  417.6 29.7 %while.169 = (s32[]{:T(128)}, f32[2,64,128]{2,1,0:T(8,128)S(1)}, f32[3,2,64,64]{3,2,1,0:T(8,128)}, f32[3,2,64,64]{3,2,1,0:T(8,128)}, f32[3,2,64,128]{3,2,0,1:T(8...) while((s32[]{:T(128)}, f32[2,64,128]{2,1,0:T(8,128)S(1)}, ...), condition=%wide.region_32.33_spmd.clone, body=%wide.region_31.32_spmd.clone.sunk | while | flops 88195072 | bytes 1894609 | solution.py:73
  424.0 1.8 fusion.339
  425.8 1.8 fusion.341
  433.9 1.8 fusion.339
  435.7 1.7 fusion.341
  442.1 1.7 fusion.338
  443.8 1.8 fusion.339
  445.6 1.8 fusion.341
  (354 shorter events, 150.3 us)
Async XLA Ops:
  7.2 67.0 %copy-start = (bf16[1,576,2048]{2,1,0:T(8,128)(2,1)S(1)}, bf16[1,576,2048]{2,1,0:T(8,128)(2,1)}, u32[]{:S(2)}) copy-start(bf16[1,576,2048]{2,1,0:T(8,128)(2,1)} %param.32) | copy-start | bytes 7077892
  22.9 8.5 %copy-start.24 = (f32[192,128]{1,0:T(8,128)S(1)}, f32[192,128]{1,0:T(8,128)}, u32[]{:S(2)}) copy-start(f32[192,128]{1,0:T(8,128)} %param.41) | copy-start | bytes 294916
  22.9 10.5 %copy-start.26 = (bf16[192,128]{1,0:T(8,128)(2,1)S(1)}, bf16[192,128]{1,0:T(8,128)(2,1)}, u32[]{:S(2)}) copy-start(bf16[192,128]{1,0:T(8,128)(2,1)} %param.38) | copy-start | bytes 147460
  23.9 10.5 %copy-start.25 = (bf16[192,256]{1,0:T(8,128)(2,1)S(1)}, bf16[192,256]{1,0:T(8,128)(2,1)}, u32[]{:S(2)}) copy-start(bf16[192,256]{1,0:T(8,128)(2,1)} %param.39) | copy-start | bytes 294916
  23.9 12.3 %copy-start.27 = (bf16[192,128]{1,0:T(8,128)(2,1)S(1)}, bf16[192,128]{1,0:T(8,128)(2,1)}, u32[]{:S(2)}) copy-start(bf16[192,128]{1,0:T(8,128)(2,1)} %param.37) | copy-start | bytes 147460
  23.9 54.8 %all-to-all-start = ((bf16[8,72,512]{2,1,0:T(8,128)(2,1)}), bf16[8,72,512]{2,1,0:T(8,128)(2,1)}, u32[]{:S(2)}, u32[]{:S(2)}) async-start(bf16[8,72,512]{2,1,0:T(8,128)(2,1)} %fusion.179), calls=%async_computation | async-start | bytes 1179648 | tf_op jit(solution)/shard_map/all_to_all | solution.py:157
  31.4 73.3 %all-gather.10.cloned.1.call-start = ((), (), s32[]{:S(2)}) async-start(), calls=%async_computation.3 | async-start | bytes 2949120 | tf_op jit(solution)/shard_map/all_gather | solution.py:164
  31.5 4.7 %copy-start.8 = (f32[192,128]{0,1:T(8,128)}, f32[192,128]{0,1:T(8,128)S(1)}, u32[]{:S(2)}) copy-start(f32[192,128]{0,1:T(8,128)S(1)} %copy.175) | copy-start | bytes 294916
  33.5 0.7 copy-start.11
  69.5 7.6 %copy-start.10 = (f32[2,64,2,128]{3,1,2,0:T(8,128)}, f32[2,64,2,128]{3,1,2,0:T(8,128)S(1)}, u32[]{:S(2)}) copy-start(f32[2,64,2,128]{3,1,2,0:T(8,128)S(1)} %reduce-window.24) | copy-start | bytes 393220
  74.2 2.9 copy-start.14
  78.7 103.8 %all-reduce.4.cloned.1.call-start = ((), (), s32[]{:S(2)}) async-start(), calls=%async_computation.4 | async-start | bytes 4718592 | tf_op jit(solution)/shard_map/psum | solution.py:195
  104.6 3.3 copy-start.12
  107.9 0.9 copy-start.7
  107.9 1.3 copy-start.15
  111.5 0.9 copy-start.9
  111.5 1.1 copy-start.28
  182.5 8.9 %copy-start.29 = (s32[384]{0:T(512)S(1)}, s32[384]{0:T(512)}, u32[]{:S(2)}) copy-start(s32[384]{0:T(512)} %get-tuple-element.1749) | copy-start | bytes 4612
  182.5 9.7 %copy-start.17 = (f32[3,2,64,128]{3,2,1,0:T(8,128)S(1)}, f32[3,2,64,128]{3,2,1,0:T(8,128)}, u32[]{:S(2)}) copy-start(f32[3,2,64,128]{3,2,1,0:T(8,128)} %get-tuple-element.1224) | copy-start | bytes 589828
  182.5 15.0 %copy-start.30 = (f32[1,2,64]{2,1,0:T(2,128)S(1)}, f32[1,2,64]{2,1,0:T(2,128)}, u32[]{:S(2)}) copy-start(f32[1,2,64]{2,1,0:T(2,128)} %exponential_bitcast_fusion.1) | copy-start | bytes 1540
  182.5 47.4 %copy-start.31 = (f32[1,2,64]{2,1,0:T(2,128)S(1)}, f32[1,2,64]{2,1,0:T(2,128)}, u32[]{:S(2)}) copy-start(f32[1,2,64]{2,1,0:T(2,128)} %exponential_bitcast_fusion) | copy-start | bytes 1540
  182.6 97.6 %all-to-all-start.1 = ((bf16[8,72,2048]{2,1,0:T(8,128)(2,1)}), bf16[8,72,2048]{2,1,0:T(8,128)(2,1)}, u32[]{:S(2)}, u32[]{:S(2)}) async-start(bf16[8,72,2048]{2,1,0:T(8,128)(2,1)} %all-reduce.4.cloned.1.call-done), calls=%async_computation.1 | async-start | bytes 4718592 | tf_op jit(solution)/shard_map/all_to_all | solution.py:196
  191.3 269.2 %reduce-scatter.2.cloned.1.call-start = ((), (), s32[]{:S(2)}) async-start(), calls=%async_computation.5 | async-start | bytes 2359296 | tf_op jit(solution)/shard_map/reduce_scatter | solution.py:237
  197.5 104.6 %copy-start.5 = (f32[2,256,64]{1,2,0:T(8,128)}, f32[2,256,64]{1,2,0:T(8,128)S(1)}, u32[]{:S(2)}) copy-start(f32[2,256,64]{1,2,0:T(8,128)S(1)} %reverse.7) | copy-start | bytes 393220
  257.7 11.0 %copy-start.2 = (f32[2,64,128]{2,1,0:T(8,128)}, f32[2,64,128]{2,1,0:T(8,128)S(1)}, u32[]{:S(2)}) copy-start(f32[2,64,128]{2,1,0:T(8,128)S(1)} %get-tuple-element.1226) | copy-start | bytes 196612
  287.2 4.8 %copy-start.21 = (f32[192,2]{1,0:T(8,128)S(1)}, f32[192,2]{1,0:T(8,128)}, u32[]{:S(2)}) copy-start(f32[192,2]{1,0:T(8,128)} %reshape.471) | copy-start | bytes 4612
  292.0 7.0 %copy-start.4 = (bf16[192,2048]{1,0:T(8,128)(2,1)S(1)}, bf16[192,2048]{1,0:T(8,128)(2,1)}, u32[]{:S(2)}) copy-start(bf16[192,2048]{1,0:T(8,128)(2,1)} %param.29) | copy-start | bytes 2359300
  292.0 7.0 %copy-start.13 = (bf16[2048,256]{1,0:T(8,128)(2,1)S(1)}, bf16[2048,256]{1,0:T(8,128)(2,1)}, u32[]{:S(2)}) copy-start(bf16[2048,256]{1,0:T(8,128)(2,1)} %param.36) | copy-start | bytes 3145732
  299.0 2.2 copy-start.1
  299.0 1.1 copy-start.16
  299.0 2.1 copy-start.6
  304.5 3.5 copy-start.23
  308.0 40.9 %copy-start.22 = (f32[2,64,128]{2,1,0:T(8,128)S(1)}, f32[2,64,128]{2,1,0:T(8,128)}, u32[]{:S(2)}) copy-start(f32[2,64,128]{2,1,0:T(8,128)} %fusion.202) | copy-start | bytes 196612
  417.6 37.4 %copy-start.3 = (f32[2,64,128]{2,1,0:T(8,128)S(1)}, f32[2,64,128]{2,1,0:T(8,128)}, u32[]{:S(2)}) copy-start(f32[2,64,128]{2,1,0:T(8,128)} %copy-done.2) | copy-start | bytes 196612
  447.3 9.9 %copy-start.19 = (f32[3,2,64,64]{3,2,1,0:T(8,128)S(1)}, f32[3,2,64,64]{3,2,1,0:T(8,128)}, u32[]{:S(2)}) copy-start(f32[3,2,64,64]{3,2,1,0:T(8,128)} %get-tuple-element.1255) | copy-start | bytes 294916
  447.3 10.3 %copy-start.18 = (f32[3,2,64,64]{3,2,1,0:T(8,128)S(1)}, f32[3,2,64,64]{3,2,1,0:T(8,128)}, u32[]{:S(2)}) copy-start(f32[3,2,64,64]{3,2,1,0:T(8,128)} %get-tuple-element.1256) | copy-start | bytes 294916
  449.0 9.5 %copy-start.20 = (f32[3,2,64,128]{3,2,0,1:T(8,128)S(1)}, f32[3,2,64,128]{3,2,0,1:T(8,128)}, u32[]{:S(2)}) copy-start(f32[3,2,64,128]{3,2,0,1:T(8,128)} %get-tuple-element.1257) | copy-start | bytes 589828
Sparse Core Ops, SparseCore 0:
  78.9 25.3 all-gather.9
  111.7 57.0 all-reduce.3
  308.1 69.2 reduce-scatter.1
where the time goes:
time: 474 us; the launch traced here: 467 us
  blocking collectives  194 us (41%)
  matrix products  106 us (22%)
  local copies, waits for them, and re-layouts  87.3 us (18%)
  other arithmetic  47.6 us (10%)
  starting transfers between devices  16.3 us (3%)
  between operations  14.5 us (3%)
    all_gather x6, blocking collectives, carried_in(): gathered = jax.tree.map(lambda a: lax.all_gather(a, axis), part)  194 us
    dot_general x18, matrix products, advance(): jnp.einsum('hik,hjk->hij', query_block * jnp.exp(running_total - middle),...  28.4 us
    another operation x41, local copies, waits for them, and re-layouts  23.3 us
    dot_general x18, matrix products, advance(): jnp.einsum('zuw,zwo->zuo', query_block * jnp.exp(running_total), carried_...  18.6 us
    dot_general x18, matrix products, advance(): jnp.einsum('xor,xot->xrt', key_block * jnp.exp(final_row - running_total)...  14.5 us
    unnamed x84, local copies, waits for them, and re-layouts  14.3 us
    add x14, other arithmetic, combine(): return (earlier[0] * later[0], later[0][:, :, None] * earlier[1] + later[1])  13.1 us
    dot_general x18, matrix products, advance(): jnp.einsum('hij,hjv->hiv', scores, value_block, precision=lax.Precision.H...  13.1 us
  transfers between devices with their start and end apart: 5, of which 0 were waited for; matrix products, arithmetic and copies ran while one was open for 40% of the time, Pallas kernels for 0%

commit v1 on v0

v1 whole, which is shorter than its diff:
```python
import functools

import jax
import jax.numpy as jnp
from jax import lax
from jax.experimental import pallas as pl
from jax.experimental.pallas import tpu as pltpu
from jax.sharding import PartitionSpec as P

KEY_CHANNELS = 64
DV = 128
BLOCK = 64
EPSILON = 1e-06
SCALE = KEY_CHANNELS ** (-0.5)
TAIL = 16
F32 = jnp.float32
BF16 = jnp.bfloat16
HIGHEST = lax.Precision.HIGHEST


def mm(a, b, contract, precision=None):
    return lax.dot_general(
        a, b, ((contract[:1], contract[1:]), ((), ())), preferred_element_type=F32, precision=precision
    )


def bmm(a, b, contract):
    return mm(a.astype(BF16), b.astype(BF16), contract)


def call(kernel, outs, cost, *args, **scratch):
    flops, nbytes = cost
    return pl.pallas_call(
        kernel,
        out_shape=outs,
        in_specs=[pl.BlockSpec(memory_space=pltpu.VMEM)] * len(args),
        out_specs=jax.tree.map(lambda _: pl.BlockSpec(memory_space=pltpu.VMEM), outs),
        cost_estimate=pl.CostEstimate(flops=flops, bytes_accessed=nbytes, transcendentals=0),
        **scratch,
    )(*args)


def iota(shape, dim):
    return lax.broadcasted_iota(jnp.int32, shape, dim)


def cumulative(fwd_ref, bwd_ref):
    length = fwd_ref.shape[0]
    row, col = iota((length, length), 0), iota((length, length), 1)
    rising = mm((col <= row).astype(F32), fwd_ref[...], (1, 0), HIGHEST)
    falling = mm((col >= row).astype(F32), bwd_ref[...], (1, 0), HIGHEST)
    return rising, falling


def head_mask(h, shape):
    return (iota(shape, 1) // KEY_CHANNELS) == h


def masked(h, array):
    return jnp.where(head_mask(h, array.shape), array, jnp.zeros_like(array))


def put_chunks(out_ref, fwd_state, bwd_state, fwd_total, bwd_total, forward_up):
    n = out_ref.shape[0]
    me = lax.axis_index("sp")
    lanes = out_ref.shape[2]

    def packed(state, total):
        hi = total.astype(BF16)
        rest = total - hi.astype(F32)
        mid = rest.astype(BF16)
        low = (rest - mid.astype(F32)).astype(BF16)
        row = iota((TAIL, lanes), 0)
        wide = lambda a: jnp.broadcast_to(a.astype(F32), (TAIL, lanes))
        tail = jnp.where(
            row == 0, wide(hi), jnp.where(row == 1, wide(mid), jnp.where(row == 2, wide(low), 0.0))
        )
        return state, tail

    fstate, ftail = packed(fwd_state, fwd_total)
    bstate, btail = packed(bwd_state, bwd_total)

    def one(d, carry):
        up = (d > me) if forward_up else (d < me)
        out_ref[pl.ds(d, 1), 0:DV, :] = jnp.where(up, fstate, bstate).astype(BF16)[None]
        out_ref[pl.ds(d, 1), DV : DV + TAIL, :] = jnp.where(up, ftail, btail).astype(BF16)[None]
        return carry

    lax.fori_loop(0, n, one, 0)


def take_chunks(in_ref):
    n, _, lanes = in_ref.shape
    me = lax.axis_index("sp")

    def piece(s):
        state = in_ref[pl.ds(s, 1), 0:DV, :][0].astype(F32)
        tail = in_ref[pl.ds(s, 1), DV : DV + TAIL, :][0].astype(F32)
        total = tail[0:1] + tail[1:2] + tail[2:3]
        return state, jnp.exp(total)

    def ahead(s, state):
        fresh, decay = piece(s)
        return jnp.where(s < me, state * decay + fresh, state)

    def behind(hop, state):
        s = n - 1 - hop
        fresh, decay = piece(s)
        return jnp.where(s > me, state * decay + fresh, state)

    zero = jnp.zeros((DV, lanes), F32)
    return lax.fori_loop(0, n, ahead, zero), lax.fori_loop(0, n, behind, zero)


def dispatch_kernel(routes_ref, weight_ref, grad_ref, out_ref, spread_ref, own_ref, *, experts, capacity):
    rows = routes_ref.shape[0]
    share = own_ref.shape[1]
    slots = experts * capacity
    wide = max(128, experts)
    tp = lax.axis_index("tp")
    lane = iota((rows, wide), 1)
    first = routes_ref[:, 0:1]
    second = routes_ref[:, 1:2]
    is_first = lane == first
    is_second = lane == second
    members = jnp.where(is_first, 1.0, 0.0) + jnp.where(is_second, 1.0, 0.0)
    row, col = iota((rows, rows), 0), iota((rows, rows), 1)
    before = bmm((col < row).astype(F32), members, (1, 0))
    slot = iota((rows, slots), 1)

    def spread(chosen, mine):
        rank = jnp.sum(jnp.where(mine, before, 0.0), axis=1, keepdims=True).astype(jnp.int32)
        target = jnp.where(rank < capacity, chosen * capacity + rank, -1)
        return jnp.where(slot == target, 1.0, 0.0)

    one = spread(first, is_first)
    two = spread(second, is_second)
    own = grad_ref[:, pl.ds(pl.multiple_of(tp * share, 128), share)]
    own_ref[...] = own
    wide_own = own.astype(F32)
    left = (wide_own * weight_ref[:, 0:1]).astype(BF16)
    right = (wide_own * weight_ref[:, 1:2]).astype(BF16)
    out_ref[...] = (bmm(one, left, (0, 0)) + bmm(two, right, (0, 0))).astype(BF16)
    spread_ref[...] = (one + two).astype(BF16)


def ends_kernel(k_ref, v_ref, fwd_ref, bwd_ref, out_ref):
    length, lanes = k_ref.shape
    rising, falling = cumulative(fwd_ref, bwd_ref)
    fwd_total = rising[length - 1 : length]
    bwd_total = falling[0:1]
    k = k_ref[...].astype(F32)
    kf = k * jnp.exp(fwd_total - rising)
    kb = k * jnp.exp(bwd_total - falling)
    fend = jnp.zeros((DV, lanes), F32)
    bend = jnp.zeros((DV, lanes), F32)
    for h in range(lanes // KEY_CHANNELS):
        v = v_ref[:, h * DV : (h + 1) * DV]
        fend = fend + bmm(v, masked(h, kf), (0, 0))
        bend = bend + bmm(v, masked(h, kb), (0, 0))
    put_chunks(out_ref, fend, bend, fwd_total, bwd_total, True)


def block_factors(b, rising, falling):
    s = b * BLOCK
    fmid = rising[s + BLOCK // 2 - 1 : s + BLOCK // 2]
    bmid = falling[s + BLOCK // 2 : s + BLOCK // 2 + 1]
    block = slice(s, s + BLOCK)
    return (
        jnp.exp(rising[block] - fmid),
        jnp.exp(jnp.minimum(fmid - rising, 64.0)),
        jnp.exp(falling[block] - bmid),
        jnp.exp(jnp.minimum(bmid - falling, 64.0)),
    )


def causal(b, length):
    return iota((BLOCK, length), 1) <= iota((BLOCK, length), 0) + b * BLOCK


def forward_kernel(in_ref, q_ref, k_ref, v_ref, fwd_ref, bwd_ref, score_ref, o_ref, rows_ref, s_ref, r_ref):
    length, lanes = q_ref.shape
    heads = lanes // KEY_CHANNELS
    entry, back_entry = take_chunks(in_ref)
    s_ref[...] = entry
    r_ref[...] = back_entry
    rising, falling = cumulative(fwd_ref, bwd_ref)
    q = q_ref[...].astype(F32) * SCALE
    k = k_ref[...].astype(F32)
    for b in range(length // BLOCK):
        block = slice(b * BLOCK, (b + 1) * BLOCK)
        fq, fk, bq, bk = block_factors(b, rising, falling)
        qf = q[block] * fq
        qb = q[block] * bq
        kf = (k * fk).astype(BF16)
        kb = (k * bk).astype(BF16)
        keep = causal(b, length)
        for h in range(heads):
            fs = bmm(masked(h, qf), kf, (1, 1))
            bs = bmm(masked(h, qb), kb, (1, 1))
            score_ref[h, block, :] = jnp.where(keep, fs, bs).astype(BF16)
    qs = q * jnp.exp(rising)
    qr = q * jnp.exp(falling)
    for h in range(heads):
        cols = slice(h * DV, (h + 1) * DV)
        o = mm(score_ref[h], v_ref[:, cols], (1, 0))
        o = o + bmm(masked(h, qs), entry, (1, 1)) + bmm(masked(h, qr), back_entry, (1, 1))
        o_ref[:, cols] = o
        rms = lax.rsqrt(jnp.mean(o * o, axis=1, keepdims=True) + EPSILON)
        rows_ref[:, cols] = (o * rms).astype(BF16)


def cotangent_kernel(*refs, parts):
    streams = refs[:parts]
    proj_ref, o_ref, q_ref, fwd_ref, bwd_ref, do_ref, out_ref = refs[parts:]
    length, lanes = q_ref.shape
    share = streams[0].shape[1]
    tp = lax.axis_index("tp")
    grad = jnp.zeros(o_ref.shape, F32)
    for m in range(parts):
        first = pl.multiple_of((tp ^ m) * share, 128)
        grad = grad + mm(streams[m][...], proj_ref[pl.ds(first, share), :], (1, 0))
    rising, falling = cumulative(fwd_ref, bwd_ref)
    q = q_ref[...].astype(F32) * SCALE
    qs = q * jnp.exp(rising)
    qr = q * jnp.exp(falling)
    ds = jnp.zeros((DV, lanes), F32)
    dr = jnp.zeros((DV, lanes), F32)
    for h in range(lanes // KEY_CHANNELS):
        cols = slice(h * DV, (h + 1) * DV)
        o = o_ref[:, cols]
        rms = lax.rsqrt(jnp.mean(o * o, axis=1, keepdims=True) + EPSILON)
        mixed = o * rms
        dm = grad[:, cols]
        do = (rms * (dm - mixed * jnp.mean(dm * mixed, axis=1, keepdims=True))).astype(BF16)
        do_ref[:, cols] = do
        ds = ds + bmm(do, masked(h, qs), (0, 0))
        dr = dr + bmm(do, masked(h, qr), (0, 0))
    put_chunks(out_ref, ds, dr, rising[length - 1 : length], falling[0:1], False)


def proj_kernel(*refs, parts):
    streams = refs[:parts]
    rows_ref, out_ref = refs[parts:]
    share = streams[0].shape[1]
    tp = lax.axis_index("tp")
    for m in range(parts):
        first = pl.multiple_of((tp ^ m) * share, 128)
        out_ref[pl.ds(first, share), :] = mm(streams[m][...], rows_ref[...], (0, 0)).astype(BF16)


def local_kernel(do_ref, score_ref, q_ref, k_ref, v_ref, fwd_ref, bwd_ref, s_ref, r_ref, dq_ref, dk_ref, dv_ref):
    length, lanes = q_ref.shape
    heads = lanes // KEY_CHANNELS
    rising, falling = cumulative(fwd_ref, bwd_ref)
    q = q_ref[...].astype(F32) * SCALE
    k = k_ref[...].astype(F32)
    dk = jnp.zeros((length, lanes), F32)
    reach = jnp.zeros((length, lanes), F32)
    reach_back = jnp.zeros((length, lanes), F32)
    for h in range(heads):
        cols = slice(h * DV, (h + 1) * DV)
        do = do_ref[:, cols]
        dv_ref[:, cols] = mm(score_ref[h], do, (0, 0))
        reach = reach + bmm(do, masked(h, s_ref[...]), (1, 0))
        reach_back = reach_back + bmm(do, masked(h, r_ref[...]), (1, 0))
    far = reach * jnp.exp(rising) + reach_back * jnp.exp(falling)
    for b in range(length // BLOCK):
        block = slice(b * BLOCK, (b + 1) * BLOCK)
        fq, fk, bq, bk = block_factors(b, rising, falling)
        qf = q[block] * fq
        qb = q[block] * bq
        kf = k * fk
        kb = k * bk
        keep = causal(b, length)
        dqf = jnp.zeros((BLOCK, lanes), F32)
        dqb = jnp.zeros((BLOCK, lanes), F32)
        dkf = jnp.zeros((length, lanes), F32)
        dkb = jnp.zeros((length, lanes), F32)
        for h in range(heads):
            cols = slice(h * DV, (h + 1) * DV)
            dscore = mm(do_ref[block, cols], v_ref[:, cols], (1, 1))
            df = jnp.where(keep, dscore, 0.0).astype(BF16)
            db = jnp.where(keep, 0.0, dscore).astype(BF16)
            dqf = dqf + bmm(df, masked(h, kf), (1, 0))
            dqb = dqb + bmm(db, masked(h, kb), (1, 0))
            dkf = dkf + bmm(df, masked(h, qf), (0, 0))
            dkb = dkb + bmm(db, masked(h, qb), (0, 0))
        dq_ref[block, :] = ((dqf * fq + dqb * bq + far[block]) * SCALE).astype(BF16)
        dk = dk + dkf * fk + dkb * bk
    dk_ref[...] = dk


def last_kernel(in_ref, k_ref, v_ref, fwd_ref, bwd_ref, dk_in, dv_in, dk_ref, dv_ref):
    length, lanes = k_ref.shape
    earlier, later = take_chunks(in_ref)
    rising, falling = cumulative(fwd_ref, bwd_ref)
    ff = jnp.exp(rising[length - 1 : length] - rising)
    bf = jnp.exp(falling[0:1] - falling)
    k = k_ref[...].astype(F32)
    kf = k * ff
    kb = k * bf
    ahead = jnp.zeros((length, lanes), F32)
    behind = jnp.zeros((length, lanes), F32)
    for h in range(lanes // KEY_CHANNELS):
        cols = slice(h * DV, (h + 1) * DV)
        v = v_ref[:, cols]
        ahead = ahead + bmm(v, masked(h, later), (1, 0))
        behind = behind + bmm(v, masked(h, earlier), (1, 0))
        dv = dv_in[:, cols] + bmm(masked(h, kf), later, (1, 1)) + bmm(masked(h, kb), earlier, (1, 1))
        dv_ref[:, cols] = dv.astype(BF16)
    dk_ref[...] = (dk_in[...] + ahead * ff + behind * bf).astype(BF16)


def exchange(array):
    return lax.all_to_all(array, "sp", split_axis=0, concat_axis=0, tiled=True)


def on_device(
    layer_grad,
    routes,
    route_weight,
    slot_tokens,
    gate_proj,
    up_proj,
    down_proj,
    out_proj,
    queries,
    keys,
    values,
    fwd_decay,
    bwd_decay,
):
    sds = jax.ShapeDtypeStruct
    devices = lax.axis_size("sp")
    parts = lax.axis_size("tp")
    tp = lax.axis_index("tp")
    rows, width = layer_grad.shape
    slots = slot_tokens.shape[1]
    capacity = slots // devices
    share = width // parts
    lanes = keys.shape[1]
    heads = lanes // KEY_CHANNELS
    vwidth = values.shape[1]

    def swap(array, bit):
        return lax.ppermute(array, "tp", [(i, i ^ bit) for i in range(parts)])

    def gather_parts(own):
        pieces = {0: own}
        bit = parts // 2
        while bit:
            for m in list(pieces):
                pieces[m ^ bit] = swap(pieces[m], bit)
            bit //= 2
        return [pieces[m] for m in range(parts)]

    outgoing, spread, own_grad = call(
        functools.partial(dispatch_kernel, experts=devices, capacity=capacity),
        (sds((slots, share), BF16), sds((rows, slots), BF16), sds((rows, share), BF16)),
        (8 * rows * slots * share, 3 << 20),
        routes,
        route_weight,
        layer_grad,
    )
    arrived = exchange(outgoing.reshape(devices, capacity, share)).reshape(slots, share)

    chunk = sds((devices, DV + TAIL, lanes), BF16)
    ends = call(ends_kernel, chunk, (2 * 10**9, 3 << 20), keys, values, fwd_decay, bwd_decay)
    inbound = gather_parts(arrived)
    states = exchange(ends)

    x = slot_tokens[0]
    w_gate, w_up, w_down = gate_proj[0], up_proj[0], down_proj[0]
    gate = jnp.dot(x, w_gate, preferred_element_type=F32)
    upper = jnp.dot(x, w_up, preferred_element_type=F32)
    sigma = jax.nn.sigmoid(gate)
    act = (gate * sigma * upper).astype(BF16)

    scores, o, mixed_rows, entry, back_entry = call(
        forward_kernel,
        (
            sds((heads, rows, rows), BF16),
            sds((rows, vwidth), F32),
            sds((rows, vwidth), BF16),
            sds((DV, lanes), F32),
            sds((DV, lanes), F32),
        ),
        (4 * 10**9, 3 << 20),
        states,
        queries,
        keys,
        values,
        fwd_decay,
        bwd_decay,
    )

    act_grad = 0.0
    for m in range(parts):
        w = lax.dynamic_slice_in_dim(w_down, (tp ^ m) * share, share, 1)
        act_grad = act_grad + mm(inbound[m], w, (1, 1))
    up_delta = (act_grad * gate * sigma).astype(BF16)
    gate_delta = (act_grad * upper * sigma * (1.0 + gate * (1.0 - sigma))).astype(BF16)

    def slot_piece(m):
        wg = lax.dynamic_slice_in_dim(w_gate, (tp ^ m) * share, share, 0)
        wu = lax.dynamic_slice_in_dim(w_up, (tp ^ m) * share, share, 0)
        return (mm(gate_delta, wg, (1, 1)) + mm(up_delta, wu, (1, 1))).astype(BF16)

    pieces = {m: slot_piece(m) for m in reversed(range(parts))}
    bit = 1
    while bit < parts:
        kept = [m for m in pieces if not m & bit]
        pieces = {
            m: (pieces[m].astype(F32) + swap(pieces[m ^ bit], bit).astype(F32)).astype(BF16)
            for m in kept
        }
        bit *= 2
    back = exchange(pieces[0].reshape(devices, capacity, share)).reshape(slots, share)

    grad_gate = mm(x, gate_delta, (0, 0)).astype(BF16)
    grad_up = mm(x, up_delta, (0, 0)).astype(BF16)
    grad_down = jnp.zeros(w_down.shape, BF16)
    for m in range(parts):
        grad_down = lax.dynamic_update_slice_in_dim(
            grad_down, mm(act, inbound[m], (0, 0)).astype(BF16), (tp ^ m) * share, 1
        )

    stream = (own_grad.astype(F32) + mm(spread, back, (1, 0))).astype(BF16)
    streams = gather_parts(stream)
    do, cots = call(
        functools.partial(cotangent_kernel, parts=parts),
        (sds((rows, vwidth), BF16), chunk),
        (2 * 10**9, 4 << 20),
        *streams,
        out_proj,
        o,
        queries,
        fwd_decay,
        bwd_decay,
    )
    cots = exchange(cots)
    term = call(
        functools.partial(proj_kernel, parts=parts),
        sds((width, vwidth), BF16),
        (2 * 10**9, 2 << 20),
        *streams,
        mixed_rows,
    )
    terms = exchange(term.reshape(devices, width // devices, vwidth))
    dq, dk_near, dv_near = call(
        local_kernel,
        (sds((rows, lanes), BF16), sds((rows, lanes), F32), sds((rows, vwidth), F32)),
        (4 * 10**9, 3 << 20),
        do,
        scores,
        queries,
        keys,
        values,
        fwd_decay,
        bwd_decay,
        entry,
        back_entry,
    )
    dk, dv = call(
        last_kernel,
        (sds((rows, lanes), BF16), sds((rows, vwidth), BF16)),
        (2 * 10**9, 3 << 20),
        cots,
        keys,
        values,
        fwd_decay,
        bwd_decay,
        dk_near,
        dv_near,
    )
    proj_grad = jnp.sum(terms.astype(F32), axis=0)
    return (grad_gate[None], grad_up[None], grad_down[None], proj_grad, dq, dk, dv)


def solution(mesh):
    placed = (
        P("sp", None),
        P("sp", None),
        P("sp", None),
        P("sp", None, None),
        P("sp", None, "tp"),
        P("sp", None, "tp"),
        P("sp", "tp", None),
        P(None, "tp"),
        P("sp", "tp"),
        P("sp", "tp"),
        P("sp", "tp"),
        P("sp", "tp"),
        P("sp", "tp"),
    )
    return jax.shard_map(
        on_device,
        mesh=mesh,
        in_specs=placed,
        out_specs=(
            P("sp", None, "tp"),
            P("sp", None, "tp"),
            P("sp", "tp", None),
            P("sp", "tp"),
            P("sp", "tp"),
            P("sp", "tp"),
            P("sp", "tp"),
        ),
        check_vma=False,
    )
```

time: 474 us -> 160 us (0.34); the launches traced: 467 us -> 159 us
  blocking collectives: 194 us -> 24 us
  matrix products: 106 us -> 21.4 us
  local copies, waits for them, and re-layouts: 87.3 us -> 10.4 us
  waiting for transfers between devices: 0.1 us -> 55.4 us
  other arithmetic: 47.6 us -> 3.15 us
  Pallas kernels: 0 us -> 21.5 us
  between operations: 14.5 us -> 0.84 us
  starting transfers between devices: 16.3 us -> 22.7 us
    all_gather x6 -> x0, blocking collectives: 194 us -> none  [carried_in(): gathered = jax.tree.map(lambda a: lax.all_gather(a, axis), part)]
    dot_general x88 -> x21, matrix products: 106 us -> 21.4 us  [the longest x19 17.8 us: mm(): lax.dot_general(a, b, ((contract[:1], contract[1:]), ((), ())), preferred...]
    ppermute x0 -> x9, waiting for transfers between devices: none -> 29.5 us  [swap(): return lax.ppermute(array, 'tp', [(i, i ^ bit) for i in range(parts)])]
    all_to_all x2 -> x4, waiting for transfers between devices: 0.01 us -> 26 us  [exchange(): return lax.all_to_all(array, 'sp', split_axis=0, concat_axis=0, tiled=True)]
    all_to_all x0 -> x1, blocking collectives: none -> 24 us  [exchange(): return lax.all_to_all(array, 'sp', split_axis=0, concat_axis=0, tiled=True)]
    another operation x41 -> x0, local copies, waits for them, and re-layouts: 23.3 us -> none
    pallas_call x0 -> x7, Pallas kernels: none -> 21.5 us  [call(): pl.pallas_call(kernel, out_shape=outs, in_specs=[pl.BlockSpec(memory_spac...]
    add x16 -> x0, other arithmetic: 14.8 us -> none  [the longest x14 13.1 us: combine(): return (earlier[0] * later[0], later[0][:, :, None] * earlier[1] + later[1])]
  transfers between devices with their start and end apart: 5 -> 13, of which waited for: 0 -> 8; matrix products, arithmetic and copies ran while one was open for 40% -> 16% of each run, Pallas kernels for 0% -> 9%
where the time goes in v1:
time: 160 us; the launch traced here: 159 us
  waiting for transfers between devices  55.4 us (35%)
  blocking collectives  24 us (15%)
  starting transfers between devices  22.7 us (14%)
  Pallas kernels  21.5 us (13%)
  matrix products  21.4 us (13%)
  local copies, waits for them, and re-layouts  10.4 us (6%)
  other arithmetic  3.15 us (2%)
    ppermute x9, waiting for transfers between devices, swap(): return lax.ppermute(array, 'tp', [(i, i ^ bit) for i in range(parts)])  29.5 us
    all_to_all x4, waiting for transfers between devices, exchange(): return lax.all_to_all(array, 'sp', split_axis=0, concat_axis=0, tiled=True)  26 us
    all_to_all x1, blocking collectives, exchange(): return lax.all_to_all(array, 'sp', split_axis=0, concat_axis=0, tiled=True)  24 us
    pallas_call x7, Pallas kernels, call(): pl.pallas_call(kernel, out_shape=outs, in_specs=[pl.BlockSpec(memory_spac...  21.5 us
    dot_general x19, matrix products, mm(): lax.dot_general(a, b, ((contract[:1], contract[1:]), ((), ())), preferred...  17.8 us
    all_to_all x4, starting transfers between devices, exchange(): return lax.all_to_all(array, 'sp', split_axis=0, concat_axis=0, tiled=True)  17.5 us
    unnamed x26, local copies, waits for them, and re-layouts  9.32 us
    ppermute x9, starting transfers between devices, swap(): return lax.ppermute(array, 'tp', [(i, i ^ bit) for i in range(parts)])  5.21 us
  transfers between devices with their start and end apart: 13, of which 8 were waited for; matrix products, arithmetic and copies ran while one was open for 16% of the time, Pallas kernels for 9%

profile of v1, /device:TPU:0, one launch (start us, length us, event | category | flops | bytes accessed | tf_op | source)
XLA Modules:
  0.0 159.5 jit_solution(3965758679412484607)
XLA Ops:
  0.6 1.6 %copy.20.routes_ref = s32[192,2]{1,0:T(8,128)} copy(s32[192,2]{0,1:T(2,128)} %param.14) | data formatting | bytes 3072 | tf_op args[1]
  2.2 1.4 copy.21.weight_ref
  3.7 3.1 %shard_map.180 = (bf16[576,512]{1,0:T(8,128)(2,1)}, bf16[192,576]{1,0:T(8,128)(2,1)}, bf16[192,512]{1,0:T(8,128)(2,1)}) custom-call(s32[192,2]{1,0:T(8,128)} %copy.20.routes_ref, f32[192,2]{1,0:T(8,128)} %copy.21.weight_ref, bf16[192,2048]{1,0:T(8,128)(2,1)} %grad_ref.1), custom_call_target="tpu_custom_call" | custom-call | flops 452984832 | bytes 3145728 | tf_op jit(solution)/shard_map/pallas_call | solution.py:33
  6.8 24.0 %all_to_all.25 = bf16[8,72,512]{2,1,0:T(8,128)(2,1)S(1)} all-to-all(bf16[8,72,512]{2,1,0:T(8,128)(2,1)} %bitcast.114), channel_id=1, replica_groups=mesh['sp'=8,'tp'=4] {'sp'}, dimensions={0} | all-to-all | bytes 1179648 | tf_op jit(solution)/shard_map/all_to_all | solution.py:316
  30.7 1.5 collective-permute-start.1
  32.2 1.6 %fusion.4 = f32[576,256]{1,0:T(8,128)} fusion(bf16[1,576,2048]{2,1,0:T(8,128)(2,1)S(1)} %copy-done, bf16[1,2048,256]{2,1,0:T(8,128)(2,1)S(1)} %copy-done.1), kind=kOutput, calls=%fused_computation.6 | convolution fusion | flops 603979776 | bytes 3997696 | tf_op jit(solution)/shard_map/dot_general | solution.py:375
  33.8 2.1 %fusion.6 = f32[576,256]{1,0:T(8,128)S(1)} fusion(bf16[1,576,2048]{2,1,0:T(8,128)(2,1)S(1)} %copy-done, bf16[1,2048,256]{2,1,0:T(8,128)(2,1)} %param.18), kind=kOutput, calls=%fused_computation.8 | convolution fusion | flops 603979776 | bytes 3997696 | tf_op jit(solution)/shard_map/dot_general | solution.py:376
  35.9 10.7 %collective-permute-done.1 = bf16[576,512]{1,0:T(8,128)(2,1)} collective-permute-done((bf16[576,512]{1,0:T(8,128)(2,1)S(1)}, bf16[576,512]{1,0:T(8,128)(2,1)}, u32[]{:S(2)}, u32[]{:S(2)}) %collective-permute-start.1) | collective-permute-done | bytes 589856 | tf_op jit(solution)/shard_map/ppermute | solution.py:347
  47.0 0.4 convolution_add_fusion.6
  47.3 1.5 convolution_add_fusion.5
  48.9 0.8 copy-done.7
  49.7 1.2 multiply_convert_fusion
  51.2 0.9 copy-done.3
  52.5 0.6 collective-permute-start.4
  53.4 0.4 fusion.10
  54.2 0.5 collective-permute-done.4
  54.7 0.3 add_convert_fusion.1
  55.0 1.6 collective-permute-start.5
  56.9 0.4 fusion.9
  57.3 13.4 %collective-permute-done.5 = bf16[576,512]{1,0:T(8,128)(2,1)S(1)} collective-permute-done((bf16[576,512]{1,0:T(8,128)(2,1)S(1)}, bf16[576,512]{1,0:T(8,128)(2,1)S(1)}, u32[]{:S(2)}, u32[]{:S(2)}) %collective-permute-start.5) | collective-permute-done | bytes 589856 | tf_op jit(solution)/shard_map/ppermute | solution.py:347
  70.7 1.1 add_convert_fusion
  71.8 4.2 %all-to-all-start.1 = ((bf16[8,72,512]{2,1,0:T(8,128)(2,1)}), bf16[8,72,512]{2,1,0:T(8,128)(2,1)}, u32[]{:S(2)}, u32[]{:S(2)}) async-start(bf16[8,72,512]{2,1,0:T(8,128)(2,1)} %bitcast.112), calls=%async_computation.1 | async-start | bytes 1179648 | tf_op jit(solution)/shard_map/all_to_all | solution.py:316
  76.0 2.5 %shard_map.181 = bf16[8,144,128]{2,1,0:T(8,128)(2,1)} custom-call(bf16[192,128]{1,0:T(8,128)(2,1)} %k_ref.7, bf16[192,256]{1,0:T(8,128)(2,1)} %v_ref.7, f32[192,128]{1,0:T(8,128)} %fwd_ref.7, f32[192,128]{1,0:T(8,128)} %bwd_ref.7), custom_call_target="tpu_custom_call" | custom-call | flops 2000000000 | bytes 3145728 | tf_op jit(solution)/shard_map/pallas_call | solution.py:33
  78.5 13.3 %all-to-all-done.1 = bf16[8,72,512]{2,1,0:T(8,128)(2,1)} async-done(((bf16[8,72,512]{2,1,0:T(8,128)(2,1)}), bf16[8,72,512]{2,1,0:T(8,128)(2,1)}, u32[]{:S(2)}, u32[]{:S(2)}) %all-to-all-start.1) | async-done | bytes 589856 | tf_op jit(solution)/shard_map/all_to_all | solution.py:316
  91.8 4.1 %all-to-all-start.2 = ((bf16[8,144,128]{2,1,0:T(8,128)(2,1)}), bf16[8,144,128]{2,1,0:T(8,128)(2,1)}, u32[]{:S(2)}, u32[]{:S(2)}) async-start(bf16[8,144,128]{2,1,0:T(8,128)(2,1)} %shard_map.181), calls=%async_computation.2 | async-start | bytes 589824 | tf_op jit(solution)/shard_map/all_to_all | solution.py:316
  95.9 2.2 %fusion.14.refs_0_ = bf16[192,512]{1,0:T(8,128)(2,1)} fusion(bf16[192,576]{1,0:T(8,128)(2,1)} %get-tuple-element.24, bf16[576,512]{1,0:T(8,128)(2,1)} %bitcast.26, bf16[192,512]{1,0:T(8,128)(2,1)} %get-tuple-element.23), kind=kOutput, calls=%fused_computation.32 | convolution fusion | flops 113541120 | bytes 1204224 | tf_op jit(solution)/shard_map/dot_general | solution.py:22
  98.1 1.5 collective-permute-start.7
  99.6 4.9 %collective-permute-done.7.refs_2_ = bf16[192,512]{1,0:T(8,128)(2,1)} collective-permute-done((bf16[192,512]{1,0:T(8,128)(2,1)}, bf16[192,512]{1,0:T(8,128)(2,1)}, u32[]{:S(2)}, u32[]{:S(2)}) %collective-permute-start.7) | collective-permute-done | bytes 196640 | tf_op jit(solution)/shard_map/ppermute | solution.py:347
  104.5 0.9 all-to-all-done.2.in_ref
  105.3 3.4 %shard_map.182 = (bf16[2,192,192]{2,1,0:T(8,128)(2,1)}, f32[192,256]{1,0:T(8,128)}, bf16[192,256]{1,0:T(8,128)(2,1)}, f32[128,128]{1,0:T(8,128)}, f32[128,128]{1,0:T(8,128)}) custom-call(bf16[8,144,128]{2,1,0:T(8,128)(2,1)} %all-to-all-done.2.in_ref, bf16[192,128]{1,0:T(8,128)(2,1)} %q_ref.3, bf16[192,128]{1,0:T(8,128)(2,1)} %k_ref.7, ...), custom_call_target="tpu_custom_call" | custom-call | flops 4000000000 | bytes 3145728 | tf_op jit(solution)/shard_map/pallas_call | solution.py:33
  108.8 3.4 %shard_map.184 = (bf16[192,256]{1,0:T(8,128)(2,1)}, bf16[8,144,128]{2,1,0:T(8,128)(2,1)}) custom-call(bf16[192,512]{1,0:T(8,128)(2,1)} %fusion.14.refs_0_, bf16[192,512]{1,0:T(8,128)(2,1)} %collective-permute-done.6.refs_1_, bf16[192,512]{1,0:T(8,128)(2,1)} %collective-permute-done.7.refs_2_, bf16[192,512]{1,0:T(8,128)(2,1)} %collective-permute-done.8.refs_3_, ...), custom_call_target="tpu_custom_call" | custom-call | flops 2000000000 | bytes 4194304 | tf_op jit(solution)/shard_map/pallas_call | solution.py:33
  112.2 4.9 %all-to-all-start.4 = ((bf16[8,144,128]{2,1,0:T(8,128)(2,1)}), bf16[8,144,128]{2,1,0:T(8,128)(2,1)}, u32[]{:S(2)}, u32[]{:S(2)}) async-start(bf16[8,144,128]{2,1,0:T(8,128)(2,1)} %get-tuple-element.32), calls=%async_computation.4 | async-start | bytes 589824 | tf_op jit(solution)/shard_map/all_to_all | solution.py:316
  117.1 2.0 %fusion = bf16[1,2048,256]{1,2,0:T(8,128)(2,1)} fusion(bf16[576,256]{1,0:T(8,128)(2,1)S(1)} %get-tuple-element.45, bf16[1,576,2048]{2,1,0:T(8,128)(2,1)S(1)} %copy-done), kind=kOutput, calls=%fused_computation.2 | convolution fusion | flops 604504064 | bytes 3702784 | tf_op jit(solution)/shard_map/dot_general | solution.py:22
  119.1 2.3 %copy.22 = bf16[1,2048,256]{2,1,0:T(8,128)(2,1)} copy(bf16[1,2048,256]{1,2,0:T(8,128)(2,1)} %fusion) | data formatting | bytes 2097152
  121.3 2.7 %shard_map.183 = bf16[2048,256]{1,0:T(8,128)(2,1)} custom-call(bf16[192,512]{1,0:T(8,128)(2,1)} %fusion.14.refs_0_, bf16[192,512]{1,0:T(8,128)(2,1)} %collective-permute-done.6.refs_1_, bf16[192,512]{1,0:T(8,128)(2,1)} %collective-permute-done.7.refs_2_, bf16[192,512]{1,0:T(8,128)(2,1)} %collective-permute-done.8.refs_3_, ...), custom_call_target="tpu_custom_call" | custom-call | flops 2000000000 | bytes 2097152 | tf_op jit(solution)/shard_map/pallas_call | solution.py:33
  124.0 3.4 %all-to-all-done.4.in_ref = bf16[8,144,128]{2,1,0:T(8,128)(2,1)} async-done(((bf16[8,144,128]{2,1,0:T(8,128)(2,1)}), bf16[8,144,128]{2,1,0:T(8,128)(2,1)}, u32[]{:S(2)}, u32[]{:S(2)}) %all-to-all-start.4) | async-done | bytes 294944 | tf_op jit(solution)/shard_map/all_to_all | solution.py:316
  127.4 4.4 %all-to-all-start.3 = ((bf16[8,256,256]{2,1,0:T(8,128)(2,1)}), bf16[8,256,256]{2,1,0:T(8,128)(2,1)}, u32[]{:S(2)}, u32[]{:S(2)}) async-start(bf16[8,256,256]{2,1,0:T(8,128)(2,1)} %bitcast.113), calls=%async_computation.3 | async-start | bytes 2097152 | tf_op jit(solution)/shard_map/all_to_all | solution.py:316
  131.9 2.0 %fusion.1 = bf16[1,2048,256]{1,2,0:T(8,128)(2,1)} fusion(bf16[576,256]{1,0:T(8,128)(2,1)S(1)} %get-tuple-element.46, bf16[1,576,2048]{2,1,0:T(8,128)(2,1)S(1)} %copy-done), kind=kOutput, calls=%fused_computation.3 | convolution fusion | flops 604504064 | bytes 3702784 | tf_op jit(solution)/shard_map/dot_general | solution.py:22
  133.8 2.3 %copy.23 = bf16[1,2048,256]{2,1,0:T(8,128)(2,1)} copy(bf16[1,2048,256]{1,2,0:T(8,128)(2,1)} %fusion.1) | data formatting | bytes 2097152
  136.1 1.1 broadcast_in_dim.20
  137.2 1.1 fusion.16
  138.3 1.1 fusion.18
  139.4 2.2 %fusion.20 = bf16[1,256,2048]{2,1,0:T(8,128)(2,1)} fusion(bf16[1,256,2048]{2,1,0:T(8,128)(2,1)} %fusion.18, s32[]{:T(128)S(6)} %select_n.10, bf16[576,256]{1,0:T(8,128)(2,1)S(1)} %copy-done.9, bf16[576,512]{1,0:T(8,128)(2,1)} %collective-permute-done.1), kind=kOutput, calls=%fused_computation.38 | convolution fusion | flops 151126016 | bytes 1146884 | tf_op jit(solution)/shard_map/dot_general | solution.py:22
  141.6 1.1 fusion.22
  142.7 3.3 %shard_map.185 = (bf16[192,128]{1,0:T(8,128)(2,1)}, f32[192,128]{1,0:T(8,128)}, f32[192,256]{1,0:T(8,128)}) custom-call(bf16[192,256]{1,0:T(8,128)(2,1)} %get-tuple-element.27.do_ref, bf16[2,192,192]{2,1,0:T(8,128)(2,1)} %get-tuple-element.28.score_ref, bf16[192,128]{1,0:T(8,128)(2,1)} %q_ref.3, bf16[192,128]{1,0:T(8,128)(2,1)} %k_ref.7, ...), custom_call_target="tpu_custom_call" | custom-call | flops 4000000000 | bytes 3145728 | tf_op jit(solution)/shard_map/pallas_call | solution.py:33
  146.0 3.0 %shard_map.186 = (bf16[192,128]{1,0:T(8,128)(2,1)}, bf16[192,256]{1,0:T(8,128)(2,1)}) custom-call(bf16[8,144,128]{2,1,0:T(8,128)(2,1)} %all-to-all-done.4.in_ref, bf16[192,128]{1,0:T(8,128)(2,1)} %k_ref.7, bf16[192,256]{1,0:T(8,128)(2,1)} %v_ref.7, f32[192,128]{1,0:T(8,128)} %fwd_ref.7, f32[192,128]{1,0:T(8,128)} %bwd_ref.7, ...), custom_call_target="tpu_custom_call" | custom-call | flops 2000000000 | bytes 3145728 | tf_op jit(solution)/shard_map/pallas_call | solution.py:33
  149.0 8.4 %all-to-all-done.3 = bf16[8,256,256]{2,1,0:T(8,128)(2,1)} async-done(((bf16[8,256,256]{2,1,0:T(8,128)(2,1)}), bf16[8,256,256]{2,1,0:T(8,128)(2,1)}, u32[]{:S(2)}, u32[]{:S(2)}) %all-to-all-start.3) | async-done | bytes 1048608 | tf_op jit(solution)/shard_map/all_to_all | solution.py:316
  157.4 2.1 %convert_reduce_fusion = f32[256,256]{1,0:T(8,128)} fusion(bf16[8,256,256]{2,1,0:T(8,128)(2,1)} %all-to-all-done.3), kind=kLoop, calls=%fused_computation.10 | loop fusion | flops 983040 | bytes 1310720 | tf_op jit(solution)/shard_map/reduce_sum | solution.py:477
  (36 shorter events, 2.2 us)
Async XLA Ops:
  0.6 31.6 %copy-start = (bf16[1,576,2048]{2,1,0:T(8,128)(2,1)S(1)}, bf16[1,576,2048]{2,1,0:T(8,128)(2,1)}, u32[]{:S(2)}) copy-start(bf16[1,576,2048]{2,1,0:T(8,128)(2,1)} %param.16) | copy-start | bytes 7077892
  6.8 25.5 %copy-start.1 = (bf16[1,2048,256]{2,1,0:T(8,128)(2,1)S(1)}, bf16[1,2048,256]{2,1,0:T(8,128)(2,1)}, u32[]{:S(2)}) copy-start(bf16[1,2048,256]{2,1,0:T(8,128)(2,1)} %param.17) | copy-start | bytes 3145732
  30.7 16.2 %collective-permute-start = (bf16[576,512]{1,0:T(8,128)(2,1)S(1)}, bf16[576,512]{1,0:T(8,128)(2,1)S(1)}, u32[]{:S(2)}, u32[]{:S(2)}) collective-permute-start(bf16[576,512]{1,0:T(8,128)(2,1)S(1)} %bitcast.108), channel_id=1, source_target_pairs={{0,1},{1,0},{2,3},{3,2},{4,5},{5,4},{6,7},{7,6},{8,9},{9,8},{10,11... | collective-permute-start | bytes 1769480 | tf_op jit(solution)/shard_map/ppermute | solution.py:347
  30.7 15.8 %collective-permute-start.1 = (bf16[576,512]{1,0:T(8,128)(2,1)S(1)}, bf16[576,512]{1,0:T(8,128)(2,1)}, u32[]{:S(2)}, u32[]{:S(2)}) collective-permute-start(bf16[576,512]{1,0:T(8,128)(2,1)S(1)} %bitcast.109), channel_id=1, source_target_pairs={{0,2},{1,3},{2,0},{3,1},{4,6},{5,7},{6,4},{7,5},{8,10},{9,11},{10,... | collective-permute-start | bytes 1769480 | tf_op jit(solution)/shard_map/ppermute | solution.py:347
  33.8 12.8 %copy-start.6 = (bf16[1,256,2048]{2,1,0:T(8,128)(2,1)S(1)}, bf16[1,256,2048]{2,1,0:T(8,128)(2,1)}, u32[]{:S(2)}) copy-start(bf16[1,256,2048]{2,1,0:T(8,128)(2,1)} %param.19) | copy-start | bytes 3145732
  46.6 2.3 %collective-permute-start.2 = (bf16[576,512]{1,0:T(8,128)(2,1)}, bf16[576,512]{1,0:T(8,128)(2,1)S(1)}, u32[]{:S(2)}, u32[]{:S(2)}) collective-permute-start(bf16[576,512]{1,0:T(8,128)(2,1)} %collective-permute-done.1), channel_id=1, source_target_pairs={{0,1},{1,0},{2,3},{3,2},{4,5},{5,4},{6,7},{7,6},{8,9},{9,8},{10,11... | collective-permute-start | bytes 1769480 | tf_op jit(solution)/shard_map/ppermute | solution.py:347
  46.9 1.9 %copy-start.4 = (bf16[576,512]{1,0:T(8,128)(2,1)}, bf16[576,512]{1,0:T(8,128)(2,1)S(1)}, u32[]{:S(2)}) copy-start(bf16[576,512]{1,0:T(8,128)(2,1)S(1)} %collective-permute-done) | copy-start | bytes 1769476
  47.3 2.4 %copy-start.10 = (f32[576,256]{1,0:T(8,128)S(1)}, f32[576,256]{1,0:T(8,128)}, u32[]{:S(2)}) copy-start(f32[576,256]{1,0:T(8,128)} %fusion.4) | copy-start | bytes 1769476
  48.8 2.0 %copy-start.2 = (bf16[1,2048,256]{2,1,0:T(8,128)(2,1)S(1)}, bf16[1,2048,256]{2,1,0:T(8,128)(2,1)}, u32[]{:S(2)}) copy-start(bf16[1,2048,256]{2,1,0:T(8,128)(2,1)} %param.17) | copy-start | bytes 3145732
  48.9 0.8 copy-start.7
  50.9 1.2 copy-start.3
  52.5 2.2 %collective-permute-start.4 = (bf16[576,512]{1,0:T(8,128)(2,1)S(1)}, bf16[576,512]{1,0:T(8,128)(2,1)S(1)}, u32[]{:S(2)}, u32[]{:S(2)}) collective-permute-start(bf16[576,512]{1,0:T(8,128)(2,1)S(1)} %fusion.13), channel_id=1, source_target_pairs={{0,1},{1,0},{2,3},{3,2},{4,5},{5,4},{6,7},{7,6},{8,9},{9,8},{10,11... | collective-permute-start | bytes 1769480 | tf_op jit(solution)/shard_map/ppermute | solution.py:347
  53.7 3.6 %collective-permute-start.3 = (bf16[576,512]{1,0:T(8,128)(2,1)S(1)}, bf16[576,512]{1,0:T(8,128)(2,1)S(1)}, u32[]{:S(2)}, u32[]{:S(2)}) collective-permute-start(bf16[576,512]{1,0:T(8,128)(2,1)S(1)} %fusion.10), channel_id=1, source_target_pairs={{0,1},{1,0},{2,3},{3,2},{4,5},{5,4},{6,7},{7,6},{8,9},{9,8},{10,11... | collective-permute-start | bytes 1769480 | tf_op jit(solution)/shard_map/ppermute | solution.py:347
  55.0 15.7 %collective-permute-start.5 = (bf16[576,512]{1,0:T(8,128)(2,1)S(1)}, bf16[576,512]{1,0:T(8,128)(2,1)S(1)}, u32[]{:S(2)}, u32[]{:S(2)}) collective-permute-start(bf16[576,512]{1,0:T(8,128)(2,1)S(1)} %add_convert_fusion.1), channel_id=1, source_target_pairs={{0,2},{1,3},{2,0},{3,1},{4,6},{5,7},{6,4},{7,5},{8,10},{9,11},{10,... | collective-permute-start | bytes 1769480 | tf_op jit(solution)/shard_map/ppermute | solution.py:347
  71.8 20.1 %all-to-all-start.1 = ((bf16[8,72,512]{2,1,0:T(8,128)(2,1)}), bf16[8,72,512]{2,1,0:T(8,128)(2,1)}, u32[]{:S(2)}, u32[]{:S(2)}) async-start(bf16[8,72,512]{2,1,0:T(8,128)(2,1)} %bitcast.112), calls=%async_computation.1 | async-start | bytes 1179648 | tf_op jit(solution)/shard_map/all_to_all | solution.py:316
  91.8 13.5 %all-to-all-start.2 = ((bf16[8,144,128]{2,1,0:T(8,128)(2,1)}), bf16[8,144,128]{2,1,0:T(8,128)(2,1)}, u32[]{:S(2)}, u32[]{:S(2)}) async-start(bf16[8,144,128]{2,1,0:T(8,128)(2,1)} %shard_map.181), calls=%async_computation.2 | async-start | bytes 589824 | tf_op jit(solution)/shard_map/all_to_all | solution.py:316
  98.1 6.4 %collective-permute-start.7 = (bf16[192,512]{1,0:T(8,128)(2,1)}, bf16[192,512]{1,0:T(8,128)(2,1)}, u32[]{:S(2)}, u32[]{:S(2)}) collective-permute-start(bf16[192,512]{1,0:T(8,128)(2,1)} %fusion.14.refs_0_), channel_id=1, source_target_pairs={{0,2},{1,3},{2,0},{3,1},{4,6},{5,7},{6,4},{7,5},{8,10},{9,11},{10,... | collective-permute-start | bytes 589832 | tf_op jit(solution)/shard_map/ppermute | solution.py:347
  99.6 9.2 %collective-permute-start.6 = (bf16[192,512]{1,0:T(8,128)(2,1)}, bf16[192,512]{1,0:T(8,128)(2,1)}, u32[]{:S(2)}, u32[]{:S(2)}) collective-permute-start(bf16[192,512]{1,0:T(8,128)(2,1)} %fusion.14.refs_0_), channel_id=1, source_target_pairs={{0,1},{1,0},{2,3},{3,2},{4,5},{5,4},{6,7},{7,6},{8,9},{9,8},{10,11... | collective-permute-start | bytes 589832 | tf_op jit(solution)/shard_map/ppermute | solution.py:347
  104.5 4.3 %collective-permute-start.8 = (bf16[192,512]{1,0:T(8,128)(2,1)}, bf16[192,512]{1,0:T(8,128)(2,1)}, u32[]{:S(2)}, u32[]{:S(2)}) collective-permute-start(bf16[192,512]{1,0:T(8,128)(2,1)} %collective-permute-done.7.refs_2_), channel_id=1, source_target_pairs={{0,1},{1,0},{2,3},{3,2},{4,5},{5,4},{6,7},{7,6},{8,9},{9,8},{10,11... | collective-permute-start | bytes 589832 | tf_op jit(solution)/shard_map/ppermute | solution.py:347
  112.2 15.2 %all-to-all-start.4 = ((bf16[8,144,128]{2,1,0:T(8,128)(2,1)}), bf16[8,144,128]{2,1,0:T(8,128)(2,1)}, u32[]{:S(2)}, u32[]{:S(2)}) async-start(bf16[8,144,128]{2,1,0:T(8,128)(2,1)} %get-tuple-element.32), calls=%async_computation.4 | async-start | bytes 589824 | tf_op jit(solution)/shard_map/all_to_all | solution.py:316
  127.4 29.9 %all-to-all-start.3 = ((bf16[8,256,256]{2,1,0:T(8,128)(2,1)}), bf16[8,256,256]{2,1,0:T(8,128)(2,1)}, u32[]{:S(2)}, u32[]{:S(2)}) async-start(bf16[8,256,256]{2,1,0:T(8,128)(2,1)} %bitcast.113), calls=%async_computation.3 | async-start | bytes 2097152 | tf_op jit(solution)/shard_map/all_to_all | solution.py:316
  133.8 3.4 %copy-start.9 = (bf16[576,256]{1,0:T(8,128)(2,1)S(1)}, bf16[576,256]{1,0:T(8,128)(2,1)}, u32[]{:S(2)}) copy-start(bf16[576,256]{1,0:T(8,128)(2,1)} %get-tuple-element.44) | copy-start | bytes 884740
  136.1 2.2 %copy-start.5 = (bf16[576,512]{1,0:T(8,128)(2,1)S(1)}, bf16[576,512]{1,0:T(8,128)(2,1)}, u32[]{:S(2)}) copy-start(bf16[576,512]{1,0:T(8,128)(2,1)} %copy-done.4) | copy-start | bytes 1769476
  138.3 3.3 %copy-start.8 = (bf16[576,512]{1,0:T(8,128)(2,1)S(1)}, bf16[576,512]{1,0:T(8,128)(2,1)}, u32[]{:S(2)}) copy-start(bf16[576,512]{1,0:T(8,128)(2,1)} %copy-done.7) | copy-start | bytes 1769476

commit v2 on v1

--- a/solution.py
+++ b/solution.py
@@ -110,6 +110,76 @@
 
     zero = jnp.zeros((DV, lanes), F32)
     return lax.fori_loop(0, n, ahead, zero), lax.fori_loop(0, n, behind, zero)
+
+
+def peers(n):
+    me = lax.axis_index("sp")
+    return me, [lax.rem(me + hop, n) for hop in range(1, n)]
+
+
+def greet(n):
+    _, others = peers(n)
+    barrier = pltpu.get_barrier_semaphore()
+    for other in others:
+        pl.semaphore_signal(
+            barrier, inc=1, device_id={"sp": other}, device_id_type=pl.DeviceIdType.MESH
+        )
+    pl.semaphore_wait(barrier, n - 1)
+
+
+def send_all(n, source, landing, send_sem, recv_sem):
+    me, others = peers(n)
+    copies = []
+    for hop, other in enumerate(others):
+        copy = pltpu.make_async_remote_copy(
+            src_ref=source.at[other],
+            dst_ref=landing.at[me],
+            send_sem=send_sem.at[hop],
+            recv_sem=recv_sem.at[hop],
+            device_id={"sp": other},
+            device_id_type=pl.DeviceIdType.MESH,
+        )
+        copy.start()
+        copies.append(copy)
+    return copies
+
+
+def keep_own(source, landing):
+    me = lax.axis_index("sp")
+    landing[pl.ds(me, 1)] = source[pl.ds(me, 1)]
+
+
+def exchange_kernel(*refs, arrays):
+    sources, landings, sems = refs[:arrays], refs[arrays : 2 * arrays], refs[2 * arrays :]
+    n = sources[0].shape[0]
+    greet(n)
+    copies = []
+    for i in range(arrays):
+        copies += send_all(n, sources[i], landings[i], sems[2 * i], sems[2 * i + 1])
+    for source, landing in zip(sources, landings):
+        keep_own(source, landing)
+    for copy in copies:
+        copy.wait()
+
+
+def sems(n, arrays):
+    return [pltpu.SemaphoreType.DMA((n - 1,)) for _ in range(2 * arrays)]
+
+
+def send_params(number):
+    return pltpu.CompilerParams(collective_id=number, has_side_effects=True)
+
+
+def exchange_many(number, *arrays):
+    n = arrays[0].shape[0]
+    return call(
+        functools.partial(exchange_kernel, arrays=len(arrays)),
+        tuple(jax.ShapeDtypeStruct(a.shape, a.dtype) for a in arrays),
+        (2 * 10**9, 8 << 20),
+        *arrays,
+        scratch_shapes=sems(n, len(arrays)),
+        compiler_params=send_params(number),
+    )
 
 
 def dispatch_kernel(routes_ref, weight_ref, grad_ref, out_ref, spread_ref, own_ref, *, experts, capacity):
@@ -212,7 +282,7 @@
 
 def cotangent_kernel(*refs, parts):
     streams = refs[:parts]
-    proj_ref, o_ref, q_ref, fwd_ref, bwd_ref, do_ref, out_ref = refs[parts:]
+    proj_ref, o_ref, q_ref, fwd_ref, bwd_ref, do_ref, out_ref, column_ref = refs[parts:]
     length, lanes = q_ref.shape
     share = streams[0].shape[1]
     tp = lax.axis_index("tp")
@@ -220,6 +290,10 @@
     for m in range(parts):
         first = pl.multiple_of((tp ^ m) * share, 128)
         grad = grad + mm(streams[m][...], proj_ref[pl.ds(first, share), :], (1, 0))
+        each = column_ref.shape[2]
+        for i in range(share // each):
+            place = (tp ^ m) * (share // each) + i
+            column_ref[pl.ds(place, 1)] = streams[m][:, i * each : (i + 1) * each][None]
     rising, falling = cumulative(fwd_ref, bwd_ref)
     q = q_ref[...].astype(F32) * SCALE
     qs = q * jnp.exp(rising)
@@ -239,17 +313,66 @@
     put_chunks(out_ref, ds, dr, rising[length - 1 : length], falling[0:1], False)
 
 
-def proj_kernel(*refs, parts):
-    streams = refs[:parts]
-    rows_ref, out_ref = refs[parts:]
-    share = streams[0].shape[1]
+def weight_kernel(x_ref, gate_ref, up_ref, gate_out, up_out):
+    gate_out[...] = mm(x_ref[...], gate_ref[...], (0, 0)).astype(BF16)
+    up_out[...] = mm(x_ref[...], up_ref[...], (0, 0)).astype(BF16)
+
+
+def weight_grads(x, gate_delta, up_delta, tile):
+    slots, width = x.shape
+    hidden = gate_delta.shape[1]
+    out = jax.ShapeDtypeStruct((width, hidden), BF16)
+    whole = pl.BlockSpec((slots, hidden), lambda i: (0, 0))
+    return pl.pallas_call(
+        weight_kernel,
+        out_shape=(out, out),
+        grid=(width // tile,),
+        in_specs=[pl.BlockSpec((slots, tile), lambda i: (0, i)), whole, whole],
+        out_specs=(pl.BlockSpec((tile, hidden), lambda i: (i, 0)),) * 2,
+        cost_estimate=pl.CostEstimate(flops=3 * 10**9, bytes_accessed=5 << 20, transcendentals=0),
+    )(x, gate_delta, up_delta)
+
+
+def down_kernel(act_ref, *refs):
+    pieces, out_ref = refs[:-1], refs[-1]
     tp = lax.axis_index("tp")
-    for m in range(parts):
+    share = pieces[0].shape[1]
+    for m, piece in enumerate(pieces):
         first = pl.multiple_of((tp ^ m) * share, 128)
-        out_ref[pl.ds(first, share), :] = mm(streams[m][...], rows_ref[...], (0, 0)).astype(BF16)
-
-
-def local_kernel(do_ref, score_ref, q_ref, k_ref, v_ref, fwd_ref, bwd_ref, s_ref, r_ref, dq_ref, dk_ref, dv_ref):
+        out_ref[:, pl.ds(first, share)] = mm(act_ref[...], piece[...], (0, 0)).astype(BF16)
+
+
+def final_kernel(
+    cot_ref,
+    column_ref,
+    mixed_ref,
+    do_ref,
+    score_ref,
+    q_ref,
+    k_ref,
+    v_ref,
+    fwd_ref,
+    bwd_ref,
+    s_ref,
+    r_ref,
+    dq_ref,
+    dk_ref,
+    dv_ref,
+    proj_ref,
+    cot_in,
+    column_in,
+    dv_near,
+    cot_send,
+    cot_recv,
+    column_send,
+    column_recv,
+):
+    n = cot_ref.shape[0]
+    greet(n)
+    cot_copies = send_all(n, cot_ref, cot_in, cot_send, cot_recv)
+    column_copies = send_all(n, column_ref, column_in, column_send, column_recv)
+    keep_own(cot_ref, cot_in)
+    keep_own(column_ref, column_in)
     length, lanes = q_ref.shape
     heads = lanes // KEY_CHANNELS
     rising, falling = cumulative(fwd_ref, bwd_ref)
@@ -261,7 +384,7 @@
     for h in range(heads):
         cols = slice(h * DV, (h + 1) * DV)
         do = do_ref[:, cols]
-        dv_ref[:, cols] = mm(score_ref[h], do, (0, 0))
+        dv_near[:, cols] = mm(score_ref[h], do, (0, 0))
         reach = reach + bmm(do, masked(h, s_ref[...]), (1, 0))
         reach_back = reach_back + bmm(do, masked(h, r_ref[...]), (1, 0))
     far = reach * jnp.exp(rising) + reach_back * jnp.exp(falling)
@@ -288,16 +411,11 @@
             dkb = dkb + bmm(db, masked(h, qb), (0, 0))
         dq_ref[block, :] = ((dqf * fq + dqb * bq + far[block]) * SCALE).astype(BF16)
         dk = dk + dkf * fk + dkb * bk
-    dk_ref[...] = dk
-
-
-def last_kernel(in_ref, k_ref, v_ref, fwd_ref, bwd_ref, dk_in, dv_in, dk_ref, dv_ref):
-    length, lanes = k_ref.shape
-    earlier, later = take_chunks(in_ref)
-    rising, falling = cumulative(fwd_ref, bwd_ref)
+    for copy in cot_copies:
+        copy.wait()
+    earlier, later = take_chunks(cot_in)
     ff = jnp.exp(rising[length - 1 : length] - rising)
     bf = jnp.exp(falling[0:1] - falling)
-    k = k_ref[...].astype(F32)
     kf = k * ff
     kb = k * bf
     ahead = jnp.zeros((length, lanes), F32)
@@ -307,9 +425,15 @@
         v = v_ref[:, cols]
         ahead = ahead + bmm(v, masked(h, later), (1, 0))
         behind = behind + bmm(v, masked(h, earlier), (1, 0))
-        dv = dv_in[:, cols] + bmm(masked(h, kf), later, (1, 1)) + bmm(masked(h, kb), earlier, (1, 1))
+        dv = dv_near[:, cols] + bmm(masked(h, kf), later, (1, 1)) + bmm(masked(h, kb), earlier, (1, 1))
         dv_ref[:, cols] = dv.astype(BF16)
-    dk_ref[...] = (dk_in[...] + ahead * ff + behind * bf).astype(BF16)
+    dk_ref[...] = (dk + ahead * ff + behind * bf).astype(BF16)
+    for copy in column_copies:
+        copy.wait()
+    total = jnp.zeros(proj_ref.shape, F32)
+    for source in range(n):
+        total = total + mm(column_in[source], mixed_ref[source], (0, 0))
+    proj_ref[...] = total
 
 
 def exchange(array):
@@ -363,12 +487,10 @@
         route_weight,
         layer_grad,
     )
-    arrived = exchange(outgoing.reshape(devices, capacity, share)).reshape(slots, share)
-
     chunk = sds((devices, DV + TAIL, lanes), BF16)
     ends = call(ends_kernel, chunk, (2 * 10**9, 3 << 20), keys, values, fwd_decay, bwd_decay)
-    inbound = gather_parts(arrived)
-    states = exchange(ends)
+    arrived, states = exchange_many(0, outgoing.reshape(devices, capacity, share), ends)
+    inbound = gather_parts(arrived.reshape(slots, share))
 
     x = slot_tokens[0]
     w_gate, w_up, w_down = gate_proj[0], up_proj[0], down_proj[0]
@@ -395,6 +517,9 @@
         bwd_decay,
     )
 
+    everyone = exchange(jnp.broadcast_to(mixed_rows[None], (devices, rows, vwidth)))
+    last = inbound[1], inbound[parts - 1], mixed_rows, gate, upper
+    inbound[1], inbound[parts - 1], mixed_rows, gate, upper = lax.optimization_barrier(last)
     act_grad = 0.0
     for m in range(parts):
         w = lax.dynamic_slice_in_dim(w_down, (tp ^ m) * share, share, 1)
@@ -411,26 +536,24 @@
     bit = 1
     while bit < parts:
         kept = [m for m in pieces if not m & bit]
-        pieces = {
-            m: (pieces[m].astype(F32) + swap(pieces[m ^ bit], bit).astype(F32)).astype(BF16)
-            for m in kept
-        }
+        got = {m: swap(pieces[m ^ bit], bit) for m in kept}
         bit *= 2
-    back = exchange(pieces[0].reshape(devices, capacity, share)).reshape(slots, share)
-
-    grad_gate = mm(x, gate_delta, (0, 0)).astype(BF16)
-    grad_up = mm(x, up_delta, (0, 0)).astype(BF16)
-    grad_down = jnp.zeros(w_down.shape, BF16)
-    for m in range(parts):
-        grad_down = lax.dynamic_update_slice_in_dim(
-            grad_down, mm(act, inbound[m], (0, 0)).astype(BF16), (tp ^ m) * share, 1
-        )
+        if bit == parts:
+            grad_gate, grad_up = weight_grads(x, gate_delta, up_delta, share)
+            grad_down = call(
+                down_kernel, sds(w_down.shape, BF16), (2 * 10**9, 4 << 20), act, *inbound
+            )
+            got[0], grad_gate, grad_up, grad_down = lax.optimization_barrier(
+                (got[0], grad_gate, grad_up, grad_down)
+            )
+        pieces = {m: (pieces[m].astype(F32) + got[m].astype(F32)).astype(BF16) for m in kept}
+    back = exchange_many(1, pieces[0].reshape(devices, capacity, share))[0].reshape(slots, share)
 
     stream = (own_grad.astype(F32) + mm(spread, back, (1, 0))).astype(BF16)
     streams = gather_parts(stream)
-    do, cots = call(
+    do, cots, columns = call(
         functools.partial(cotangent_kernel, parts=parts),
-        (sds((rows, vwidth), BF16), chunk),
+        (sds((rows, vwidth), BF16), chunk, sds((devices, rows, width // devices), BF16)),
         (2 * 10**9, 4 << 20),
         *streams,
         out_proj,
@@ -439,19 +562,18 @@
         fwd_decay,
         bwd_decay,
     )
-    cots = exchange(cots)
-    term = call(
-        functools.partial(proj_kernel, parts=parts),
-        sds((width, vwidth), BF16),
-        (2 * 10**9, 2 << 20),
-        *streams,
-        mixed_rows,
-    )
-    terms = exchange(term.reshape(devices, width // devices, vwidth))
-    dq, dk_near, dv_near = call(
-        local_kernel,
-        (sds((rows, lanes), BF16), sds((rows, lanes), F32), sds((rows, vwidth), F32)),
-        (4 * 10**9, 3 << 20),
+    dq, dk, dv, proj_grad = call(
+        final_kernel,
+        (
+            sds((rows, lanes), BF16),
+            sds((rows, lanes), BF16),
+            sds((rows, vwidth), BF16),
+            sds((width // devices, vwidth), F32),
+        ),
+        (4 * 10**9, 8 << 20),
+        cots,
+        columns,
+        everyone,
         do,
         scores,
         queries,
@@ -461,20 +583,14 @@
         bwd_decay,
         entry,
         back_entry,
-    )
-    dk, dv = call(
-        last_kernel,
-        (sds((rows, lanes), BF16), sds((rows, vwidth), BF16)),
-        (2 * 10**9, 3 << 20),
-        cots,
-        keys,
-        values,
-        fwd_decay,
-        bwd_decay,
-        dk_near,
-        dv_near,
-    )
-    proj_grad = jnp.sum(terms.astype(F32), axis=0)
+        scratch_shapes=[
+            pltpu.VMEM(cots.shape, BF16),
+            pltpu.VMEM(columns.shape, BF16),
+            pltpu.VMEM((rows, vwidth), F32),
+        ]
+        + sems(devices, 2),
+        compiler_params=send_params(2),
+    )
     return (grad_gate[None], grad_up[None], grad_down[None], proj_grad, dq, dk, dv)
 
 

time: 160 us -> 155 us (0.969)
  the two profiles are of different devices: /device:TPU:0 before, /device:TPU:14 now
where the time goes in v2:
time: 155 us; the launch traced here: 154 us
  Pallas kernels  95.7 us (62%)
  matrix products  20.3 us (13%)
  waiting for transfers between devices  16.5 us (11%)
  local copies, waits for them, and re-layouts  12.6 us (8%)
  starting transfers between devices  8.24 us (5%)
    pallas_call x8, Pallas kernels, call(): pl.pallas_call(kernel, out_shape=outs, in_specs=[pl.BlockSpec(memory_spac...  90.4 us
    ppermute x9, waiting for transfers between devices, swap(): return lax.ppermute(array, 'tp', [(i, i ^ bit) for i in range(parts)])  16.5 us
    dot_general x13, matrix products, mm(): lax.dot_general(a, b, ((contract[:1], contract[1:]), ((), ())), preferred...  14.5 us
    unnamed x36, local copies, waits for them, and re-layouts  10.6 us
    all_to_all x1, starting transfers between devices, exchange(): return lax.all_to_all(array, 'sp', split_axis=0, concat_axis=0, tiled=True)  5.91 us
    pallas_call x1, Pallas kernels, weight_grads(): pl.pallas_call(weight_kernel, out_shape=(out, out), grid=(width // tile,)...  5.27 us
    dot_general x1, matrix products, on_device(): upper = jnp.dot(x, w_up, preferred_element_type=F32)  3.26 us
  transfers between devices with their start and end apart: 10, of which 4 were waited for; matrix products, arithmetic and copies ran while one was open for 14% of the time, Pallas kernels for 22%

profile of v2, /device:TPU:14, one launch (start us, length us, event | category | flops | bytes accessed | tf_op | source)
XLA Modules:
  0.0 154.2 jit_solution(16155485982371574339)
XLA Ops:
  0.6 0.0 copy-start
  0.6 1.5 copy.20.routes_ref
  2.2 1.4 copy.21.weight_ref
  3.6 3.1 %shard_map.180 = (bf16[576,512]{1,0:T(8,128)(2,1)}, bf16[192,576]{1,0:T(8,128)(2,1)}, bf16[192,512]{1,0:T(8,128)(2,1)}) custom-call(s32[192,2]{1,0:T(8,128)} %copy.20.routes_ref, f32[192,2]{1,0:T(8,128)} %copy.21.weight_ref, bf16[192,2048]{1,0:T(8,128)(2,1)} %grad_ref.1), custom_call_target="tpu_custom_call" | custom-call | flops 452984832 | bytes 3145728 | tf_op jit(solution)/shard_map/pallas_call | solution.py:33
  6.7 2.5 %shard_map.181.refs_1_ = bf16[8,144,128]{2,1,0:T(8,128)(2,1)} custom-call(bf16[192,128]{1,0:T(8,128)(2,1)} %k_ref.5, bf16[192,256]{1,0:T(8,128)(2,1)} %v_ref.5, f32[192,128]{1,0:T(8,128)} %fwd_ref.5, f32[192,128]{1,0:T(8,128)} %bwd_ref.5), custom_call_target="tpu_custom_call" | custom-call | flops 2000000000 | bytes 3145728 | tf_op jit(solution)/shard_map/pallas_call | solution.py:33
  9.2 25.8 %shard_map.182 = (bf16[8,72,512]{2,1,0:T(8,128)(2,1)}, bf16[8,144,128]{2,1,0:T(8,128)(2,1)}) custom-call(bf16[8,72,512]{2,1,0:T(8,128)(2,1)} %bitcast.84, bf16[8,144,128]{2,1,0:T(8,128)(2,1)} %shard_map.181.refs_1_), custom_call_target="tpu_custom_call" | custom-call | flops 2000000000 | bytes 8388608 | tf_op jit(solution)/shard_map/pallas_call | solution.py:33
  35.0 0.6 collective-permute-start.1
  35.6 3.4 %shard_map.183 = (bf16[2,192,192]{2,1,0:T(8,128)(2,1)}, f32[192,256]{1,0:T(8,128)}, bf16[192,256]{1,0:T(8,128)(2,1)}, f32[128,128]{1,0:T(8,128)}, f32[128,128]{1,0:T(8,128)}) custom-call(bf16[8,144,128]{2,1,0:T(8,128)(2,1)} %get-tuple-element.36.in_ref, bf16[192,128]{1,0:T(8,128)(2,1)} %q_ref.3, bf16[192,128]{1,0:T(8,128)(2,1)} %k_ref.5, ...), custom_call_target="tpu_custom_call" | custom-call | flops 4000000000 | bytes 3145728 | tf_op jit(solution)/shard_map/pallas_call | solution.py:33
  39.1 1.9 %broadcast_in_dim.18 = bf16[8,192,256]{2,1,0:T(8,128)(2,1)} broadcast(bf16[192,256]{1,0:T(8,128)(2,1)} %get-tuple-element.37), dimensions={1,2} | broadcast | bytes 884736 | tf_op jit(solution)/shard_map/broadcast_in_dim | solution.py:520
  41.0 5.9 %all-to-all-start = ((bf16[8,192,256]{2,1,0:T(8,128)(2,1)}), bf16[8,192,256]{2,1,0:T(8,128)(2,1)S(1)}, u32[]{:S(2)}, u32[]{:S(2)}) async-start(bf16[8,192,256]{2,1,0:T(8,128)(2,1)} %broadcast_in_dim.18), calls=%async_computation | async-start | bytes 1572864 | tf_op jit(solution)/shard_map/all_to_all | solution.py:440
  46.9 3.8 %collective-permute-done.1.refs_2_ = bf16[576,512]{1,0:T(8,128)(2,1)} collective-permute-done((bf16[576,512]{1,0:T(8,128)(2,1)}, bf16[576,512]{1,0:T(8,128)(2,1)}, u32[]{:S(2)}, u32[]{:S(2)}) %collective-permute-start.1) | collective-permute-done | bytes 589856 | tf_op jit(solution)/shard_map/ppermute | solution.py:471
  50.7 3.3 %fusion.7 = f32[576,256]{1,0:T(8,128)} fusion(bf16[1,2048,256]{2,1,0:T(8,128)(2,1)S(1)} %copy-done.4, bf16[1,576,2048]{2,1,0:T(8,128)(2,1)} %param.16), kind=kOutput, calls=%fused_computation.18 | convolution fusion | flops 603979776 | bytes 3997696 | tf_op jit(solution)/shard_map/dot_general | solution.py:498
  53.9 1.3 fusion.30
  55.2 0.0 copy-start.6
  55.3 2.5 %fusion.9 = f32[576,256]{1,0:T(8,128)S(1)} fusion(bf16[1,2048,256]{2,1,0:T(8,128)(2,1)S(1)} %copy-done, bf16[1,576,2048]{2,1,0:T(8,128)(2,1)} %param.16), kind=kOutput, calls=%fused_computation.20 | convolution fusion | flops 603979776 | bytes 3997696 | tf_op jit(solution)/shard_map/dot_general | solution.py:497
  57.8 0.0 collective-permute-done.refs_1_
  57.8 1.4 convolution_add_fusion.6
  59.2 0.0 copy-start.14
  59.3 1.5 convolution_add_fusion.5
  60.8 2.3 %multiply_convert_fusion.1 = (bf16[576,256]{1,0:T(8,128)(2,1)S(1)}, bf16[576,256]{1,0:T(8,128)(2,1)S(1)}, bf16[576,256]{1,0:T(8,128)(2,1)}) fusion(f32[576,256]{1,0:T(8,128)S(1)} %fusion.9, f32[576,256]{1,0:T(8,128)S(1)} %copy-done.14, f32[576,256]{1,0:T(8,128)S(1)} %convolution_add_fusion.5, bf16[576,512]{1,0:T(8,128)(2,1)} %collective-permute-done.2.refs_3_, ...), kind=kOutput, calls=%fused_computation.23 | convolution fusion | flops 153501696 | bytes 3506180 | tf_op jit(solution)/shard_map/dot_general | solution.py:22
  63.0 0.3 fusion.20
  63.4 0.4 fusion.2
  63.7 0.6 collective-permute-start.3
  64.3 0.3 fusion.12
  64.7 1.2 fusion.5
  65.9 0.0 collective-permute-start.5
  65.9 0.3 fusion.25
  66.2 1.2 add_convert_fusion.2
  67.4 0.5 collective-permute-start.4
  68.0 0.3 fusion.17
  68.3 5.3 %shard_map.184 = (bf16[2048,256]{1,0:T(8,128)(2,1)}, bf16[2048,256]{1,0:T(8,128)(2,1)}) custom-call(bf16[576,2048]{1,0:T(8,128)(2,1)} %bitcast.80, bf16[576,256]{1,0:T(8,128)(2,1)} %copy-done.3, bf16[576,256]{1,0:T(8,128)(2,1)} %copy-done.1), custom_call_target="tpu_custom_call" | custom-call | flops 3000000000 | bytes 5242880 | tf_op jit(solution)/shard_map/pallas_call | solution.py:326
  73.6 3.7 %shard_map.185 = bf16[256,2048]{1,0:T(8,128)(2,1)} custom-call(bf16[576,256]{1,0:T(8,128)(2,1)} %get-tuple-element.63.act_ref, bf16[576,512]{1,0:T(8,128)(2,1)} %bitcast.76, bf16[576,512]{1,0:T(8,128)(2,1)} %collective-permute-done.refs_1_, bf16[576,512]{1,0:T(8,128)(2,1)} %collective-permute-done.1.refs_2_, bf16[576,512]{1,0:T(8,128)(2,1)} %collective-permute-done.2.refs_3_), custom_call_target="tpu_custom_call" | custom-call | flops 2000000000 | bytes 4194304 | tf_op jit(solution)/shard_map/pallas_call | solution.py:33
  77.3 6.2 %collective-permute-done.4 = bf16[576,512]{1,0:T(8,128)(2,1)} collective-permute-done((bf16[576,512]{1,0:T(8,128)(2,1)}, bf16[576,512]{1,0:T(8,128)(2,1)}, u32[]{:S(2)}, u32[]{:S(2)}) %collective-permute-start.4) | collective-permute-done | bytes 589856 | tf_op jit(solution)/shard_map/ppermute | solution.py:471
  83.5 2.6 %add_convert_fusion = bf16[576,512]{1,0:T(8,128)(2,1)} fusion(bf16[576,512]{1,0:T(8,128)(2,1)} %collective-permute-done.4, bf16[576,512]{1,0:T(8,128)(2,1)} %collective-permute-done.5, f32[576,512]{1,0:T(8,128)S(1)} %fusion.17, bf16[576,256]{1,0:T(8,128)(2,1)S(1)} %copy-done.2, bf16[1,2048,256]{2,1,0:T(8,128)(2,1)} %param.18, s32[]{:T(128)S(6)} %select_n.8), kind=kOutput, calls=%fused_computation.14 | convolution fusion | flops 153944064 | bytes 3506180 | tf_op jit(solution)/shard_map/dot_general | solution.py:22
  86.1 17.9 %shard_map.186 = bf16[8,72,512]{2,1,0:T(8,128)(2,1)} custom-call(bf16[8,72,512]{2,1,0:T(8,128)(2,1)} %bitcast.79), custom_call_target="tpu_custom_call" | custom-call | flops 2000000000 | bytes 8388608 | tf_op jit(solution)/shard_map/pallas_call | solution.py:33
  104.0 1.4 fusion.6.refs_0_
  105.4 0.0 copy-start.10
  105.4 0.6 collective-permute-start.7
  106.0 5.1 %collective-permute-done.7.refs_2_ = bf16[192,512]{1,0:T(8,128)(2,1)S(1)} collective-permute-done((bf16[192,512]{1,0:T(8,128)(2,1)S(1)}, bf16[192,512]{1,0:T(8,128)(2,1)S(1)}, u32[]{:S(2)}, u32[]{:S(2)}) %collective-permute-start.7) | collective-permute-done | bytes 196640 | tf_op jit(solution)/shard_map/ppermute | solution.py:471
  111.1 1.4 collective-permute-done.8.refs_3_
  112.6 0.7 copy-done.13
  113.2 3.8 %shard_map.187 = (bf16[192,256]{1,0:T(8,128)(2,1)}, bf16[8,144,128]{2,1,0:T(8,128)(2,1)}, bf16[8,192,256]{2,1,0:T(8,128)(2,1)}) custom-call(bf16[192,512]{1,0:T(8,128)(2,1)} %copy-done.10, bf16[192,512]{1,0:T(8,128)(2,1)} %copy-done.12, bf16[192,512]{1,0:T(8,128)(2,1)} %copy-done.11, bf16[192,512]{1,0:T(8,128)(2,1)} %copy-done.13, ...), custom_call_target="tpu_custom_call" | custom-call | flops 2000000000 | bytes 4194304 | tf_op jit(solution)/shard_map/pallas_call | solution.py:33
  117.0 0.9 copy-done.5
  117.9 30.3 %shard_map.188 = (bf16[192,128]{1,0:T(8,128)(2,1)}, bf16[192,128]{1,0:T(8,128)(2,1)}, bf16[192,256]{1,0:T(8,128)(2,1)}, f32[256,256]{1,0:T(8,128)}) custom-call(bf16[8,144,128]{2,1,0:T(8,128)(2,1)} %get-tuple-element.51.cot_ref, bf16[8,192,256]{2,1,0:T(8,128)(2,1)} %get-tuple-element.52.column_ref, bf16[8,192,256]{2,1,0:T(8,128)(2,1)} %copy-done.5, ...), custom_call_target="tpu_custom_call" | custom-call | flops 4000000000 | bytes 8388608 | tf_op jit(solution)/shard_map/pallas_call | solution.py:33
  148.2 1.7 %copy.26 = f32[256,256]{1,0:T(8,128)} copy(f32[256,256]{1,0:T(8,128)} %get-tuple-element.74) | data formatting | bytes 524288
  149.8 1.4 copy.27
  151.3 1.4 copy.28
  152.7 1.5 copy.29
  (33 shorter events, 0.1 us)
Async XLA Ops:
  0.6 54.6 %copy-start = (bf16[1,2048,256]{2,1,0:T(8,128)(2,1)S(1)}, bf16[1,2048,256]{2,1,0:T(8,128)(2,1)}, u32[]{:S(2)}) copy-start(bf16[1,2048,256]{2,1,0:T(8,128)(2,1)} %param.17) | copy-start | bytes 3145732
  35.0 15.6 %collective-permute-start.1 = (bf16[576,512]{1,0:T(8,128)(2,1)}, bf16[576,512]{1,0:T(8,128)(2,1)}, u32[]{:S(2)}, u32[]{:S(2)}) collective-permute-start(bf16[576,512]{1,0:T(8,128)(2,1)} %bitcast.74), channel_id=1, source_target_pairs={{0,2},{1,3},{2,0},{3,1},{4,6},{5,7},{6,4},{7,5},{8,10},{9,11},{10,... | collective-permute-start | bytes 1769480 | tf_op jit(solution)/shard_map/ppermute | solution.py:471
  35.6 22.2 %collective-permute-start = (bf16[576,512]{1,0:T(8,128)(2,1)}, bf16[576,512]{1,0:T(8,128)(2,1)}, u32[]{:S(2)}, u32[]{:S(2)}) collective-permute-start(bf16[576,512]{1,0:T(8,128)(2,1)} %bitcast.75), channel_id=1, source_target_pairs={{0,1},{1,0},{2,3},{3,2},{4,5},{5,4},{6,7},{7,6},{8,9},{9,8},{10,11... | collective-permute-start | bytes 1769480 | tf_op jit(solution)/shard_map/ppermute | solution.py:471
  39.1 11.6 %copy-start.4 = (bf16[1,2048,256]{2,1,0:T(8,128)(2,1)S(1)}, bf16[1,2048,256]{2,1,0:T(8,128)(2,1)}, u32[]{:S(2)}) copy-start(bf16[1,2048,256]{2,1,0:T(8,128)(2,1)} %param.18) | copy-start | bytes 3145732
  41.0 76.0 %all-to-all-start = ((bf16[8,192,256]{2,1,0:T(8,128)(2,1)}), bf16[8,192,256]{2,1,0:T(8,128)(2,1)S(1)}, u32[]{:S(2)}, u32[]{:S(2)}) async-start(bf16[8,192,256]{2,1,0:T(8,128)(2,1)} %broadcast_in_dim.18), calls=%async_computation | async-start | bytes 1572864 | tf_op jit(solution)/shard_map/all_to_all | solution.py:440
  46.9 7.0 %copy-start.7 = (bf16[8,72,512]{2,1,0:T(8,128)(2,1)S(1)}, bf16[8,72,512]{2,1,0:T(8,128)(2,1)}, u32[]{:S(2)}) copy-start(bf16[8,72,512]{2,1,0:T(8,128)(2,1)} %get-tuple-element.35) | copy-start | bytes 1769476
  50.7 7.1 %collective-permute-start.2 = (bf16[576,512]{1,0:T(8,128)(2,1)}, bf16[576,512]{1,0:T(8,128)(2,1)}, u32[]{:S(2)}, u32[]{:S(2)}) collective-permute-start(bf16[576,512]{1,0:T(8,128)(2,1)} %collective-permute-done.1.refs_2_), channel_id=1, source_target_pairs={{0,1},{1,0},{2,3},{3,2},{4,5},{5,4},{6,7},{7,6},{8,9},{9,8},{10,11... | collective-permute-start | bytes 1769480 | tf_op jit(solution)/shard_map/ppermute | solution.py:471
  55.2 2.6 %copy-start.6 = (bf16[1,256,2048]{2,1,0:T(8,128)(2,1)S(1)}, bf16[1,256,2048]{2,1,0:T(8,128)(2,1)}, u32[]{:S(2)}) copy-start(bf16[1,256,2048]{2,1,0:T(8,128)(2,1)} %param.19) | copy-start | bytes 3145732
  59.2 1.5 copy-start.14
  63.0 3.2 %copy-start.1 = (bf16[576,256]{1,0:T(8,128)(2,1)}, bf16[576,256]{1,0:T(8,128)(2,1)S(1)}, u32[]{:S(2)}) copy-start(bf16[576,256]{1,0:T(8,128)(2,1)S(1)} %get-tuple-element.61.up_ref) | copy-start | bytes 884740
  63.0 4.9 %copy-start.3 = (bf16[576,256]{1,0:T(8,128)(2,1)}, bf16[576,256]{1,0:T(8,128)(2,1)S(1)}, u32[]{:S(2)}) copy-start(bf16[576,256]{1,0:T(8,128)(2,1)S(1)} %get-tuple-element.62.gate_ref) | copy-start | bytes 884740
  63.7 2.5 %collective-permute-start.3 = (bf16[576,512]{1,0:T(8,128)(2,1)S(1)}, bf16[576,512]{1,0:T(8,128)(2,1)S(1)}, u32[]{:S(2)}, u32[]{:S(2)}) collective-permute-start(bf16[576,512]{1,0:T(8,128)(2,1)S(1)} %fusion.2), channel_id=1, source_target_pairs={{0,1},{1,0},{2,3},{3,2},{4,5},{5,4},{6,7},{7,6},{8,9},{9,8},{10,11... | collective-permute-start | bytes 1769480 | tf_op jit(solution)/shard_map/ppermute | solution.py:471
  65.9 17.6 %collective-permute-start.5 = (bf16[576,512]{1,0:T(8,128)(2,1)}, bf16[576,512]{1,0:T(8,128)(2,1)}, u32[]{:S(2)}, u32[]{:S(2)}) collective-permute-start(bf16[576,512]{1,0:T(8,128)(2,1)} %fusion.5), channel_id=1, source_target_pairs={{0,1},{1,0},{2,3},{3,2},{4,5},{5,4},{6,7},{7,6},{8,9},{9,8},{10,11... | collective-permute-start | bytes 1769480 | tf_op jit(solution)/shard_map/ppermute | solution.py:471
  67.4 16.0 %collective-permute-start.4 = (bf16[576,512]{1,0:T(8,128)(2,1)}, bf16[576,512]{1,0:T(8,128)(2,1)}, u32[]{:S(2)}, u32[]{:S(2)}) collective-permute-start(bf16[576,512]{1,0:T(8,128)(2,1)} %add_convert_fusion.2), channel_id=1, source_target_pairs={{0,2},{1,3},{2,0},{3,1},{4,6},{5,7},{6,4},{7,5},{8,10},{9,11},{10,... | collective-permute-start | bytes 1769480 | tf_op jit(solution)/shard_map/ppermute | solution.py:471
  73.6 9.9 %copy-start.2 = (bf16[576,256]{1,0:T(8,128)(2,1)S(1)}, bf16[576,256]{1,0:T(8,128)(2,1)}, u32[]{:S(2)}) copy-start(bf16[576,256]{1,0:T(8,128)(2,1)} %copy-done.1) | copy-start | bytes 884740
  86.1 17.9 %copy-start.8 = (bf16[192,576]{1,0:T(8,128)(2,1)S(1)}, bf16[192,576]{1,0:T(8,128)(2,1)}, u32[]{:S(2)}) copy-start(bf16[192,576]{1,0:T(8,128)(2,1)} %get-tuple-element.48) | copy-start | bytes 663556
  86.1 17.9 %copy-start.9 = (bf16[192,512]{1,0:T(8,128)(2,1)S(1)}, bf16[192,512]{1,0:T(8,128)(2,1)}, u32[]{:S(2)}) copy-start(bf16[192,512]{1,0:T(8,128)(2,1)} %get-tuple-element.47) | copy-start | bytes 589828
  105.4 7.2 %copy-start.10 = (bf16[192,512]{1,0:T(8,128)(2,1)}, bf16[192,512]{1,0:T(8,128)(2,1)S(1)}, u32[]{:S(2)}) copy-start(bf16[192,512]{1,0:T(8,128)(2,1)S(1)} %fusion.6.refs_0_) | copy-start | bytes 589828
  105.4 5.7 %collective-permute-start.7 = (bf16[192,512]{1,0:T(8,128)(2,1)S(1)}, bf16[192,512]{1,0:T(8,128)(2,1)S(1)}, u32[]{:S(2)}, u32[]{:S(2)}) collective-permute-start(bf16[192,512]{1,0:T(8,128)(2,1)S(1)} %fusion.6.refs_0_), channel_id=1, source_target_pairs={{0,2},{1,3},{2,0},{3,1},{4,6},{5,7},{6,4},{7,5},{8,10},{9,11},{10,... | collective-permute-start | bytes 589832 | tf_op jit(solution)/shard_map/ppermute | solution.py:471
  106.0 5.1 %collective-permute-start.6 = (bf16[192,512]{1,0:T(8,128)(2,1)S(1)}, bf16[192,512]{1,0:T(8,128)(2,1)S(1)}, u32[]{:S(2)}, u32[]{:S(2)}) collective-permute-start(bf16[192,512]{1,0:T(8,128)(2,1)S(1)} %fusion.6.refs_0_), channel_id=1, source_target_pairs={{0,1},{1,0},{2,3},{3,2},{4,5},{5,4},{6,7},{7,6},{8,9},{9,8},{10,11... | collective-permute-start | bytes 589832 | tf_op jit(solution)/shard_map/ppermute | solution.py:471
  111.1 1.5 copy-start.11
  111.1 1.4 collective-permute-start.8
  111.1 1.4 copy-start.12
  112.6 0.7 copy-start.13
  117.0 0.9 copy-start.5

commit v3 on v2

--- a/solution.py
+++ b/solution.py
@@ -117,14 +117,14 @@
     return me, [lax.rem(me + hop, n) for hop in range(1, n)]
 
 
-def greet(n):
+def greet(n, more=0):
     _, others = peers(n)
     barrier = pltpu.get_barrier_semaphore()
     for other in others:
         pl.semaphore_signal(
             barrier, inc=1, device_id={"sp": other}, device_id_type=pl.DeviceIdType.MESH
         )
-    pl.semaphore_wait(barrier, n - 1)
+    pl.semaphore_wait(barrier, n - 1 + more)
 
 
 def send_all(n, source, landing, send_sem, recv_sem):
@@ -277,7 +277,9 @@
         o = o + bmm(masked(h, qs), entry, (1, 1)) + bmm(masked(h, qr), back_entry, (1, 1))
         o_ref[:, cols] = o
         rms = lax.rsqrt(jnp.mean(o * o, axis=1, keepdims=True) + EPSILON)
-        rows_ref[:, cols] = (o * rms).astype(BF16)
+        mixed = (o * rms).astype(BF16)
+        for d in range(rows_ref.shape[0]):
+            rows_ref[d, :, cols] = mixed
 
 
 def cotangent_kernel(*refs, parts):
@@ -287,13 +289,15 @@
     share = streams[0].shape[1]
     tp = lax.axis_index("tp")
     grad = jnp.zeros(o_ref.shape, F32)
+    part = column_ref.shape[1]
+    mine = pl.ds(pl.multiple_of(tp * part, 16), part)
     for m in range(parts):
         first = pl.multiple_of((tp ^ m) * share, 128)
         grad = grad + mm(streams[m][...], proj_ref[pl.ds(first, share), :], (1, 0))
         each = column_ref.shape[2]
         for i in range(share // each):
             place = (tp ^ m) * (share // each) + i
-            column_ref[pl.ds(place, 1)] = streams[m][:, i * each : (i + 1) * each][None]
+            column_ref[pl.ds(place, 1)] = streams[m][mine, i * each : (i + 1) * each][None]
     rising, falling = cumulative(fwd_ref, bwd_ref)
     q = q_ref[...].astype(F32) * SCALE
     qs = q * jnp.exp(rising)
@@ -366,9 +370,19 @@
     cot_recv,
     column_send,
     column_recv,
+    gather_in,
+    gather_send,
+    gather_recv,
 ):
     n = cot_ref.shape[0]
-    greet(n)
+    parts, _, part, each = gather_in.shape
+    tp = lax.axis_index("tp")
+    barrier = pltpu.get_barrier_semaphore()
+    for m in range(1, parts):
+        pl.semaphore_signal(
+            barrier, inc=1, device_id={"tp": tp ^ m}, device_id_type=pl.DeviceIdType.MESH
+        )
+    greet(n, parts - 1)
     cot_copies = send_all(n, cot_ref, cot_in, cot_send, cot_recv)
     column_copies = send_all(n, column_ref, column_in, column_send, column_recv)
     keep_own(cot_ref, cot_in)
@@ -413,6 +427,20 @@
         dk = dk + dkf * fk + dkb * bk
     for copy in cot_copies:
         copy.wait()
+    for copy in column_copies:
+        copy.wait()
+    relays = []
+    for m in range(1, parts):
+        copy = pltpu.make_async_remote_copy(
+            src_ref=column_in,
+            dst_ref=gather_in.at[tp],
+            send_sem=gather_send.at[m - 1],
+            recv_sem=gather_recv.at[m - 1],
+            device_id={"tp": tp ^ m},
+            device_id_type=pl.DeviceIdType.MESH,
+        )
+        copy.start()
+        relays.append(copy)
     earlier, later = take_chunks(cot_in)
     ff = jnp.exp(rising[length - 1 : length] - rising)
     bf = jnp.exp(falling[0:1] - falling)
@@ -428,11 +456,16 @@
         dv = dv_near[:, cols] + bmm(masked(h, kf), later, (1, 1)) + bmm(masked(h, kb), earlier, (1, 1))
         dv_ref[:, cols] = dv.astype(BF16)
     dk_ref[...] = (dk + ahead * ff + behind * bf).astype(BF16)
-    for copy in column_copies:
-        copy.wait()
     total = jnp.zeros(proj_ref.shape, F32)
-    for source in range(n):
-        total = total + mm(column_in[source], mixed_ref[source], (0, 0))
+    for m in range(parts):
+        if m:
+            relays[m - 1].wait()
+            block = gather_in[tp ^ m]
+        else:
+            block = column_in[...]
+        place = pl.ds(pl.multiple_of((tp ^ m) * part, 16), part)
+        rows = mixed_ref[:, place, :].reshape(n * part, mixed_ref.shape[2])
+        total = total + mm(block.reshape(n * part, each), rows, (0, 0))
     proj_ref[...] = total
 
 
@@ -489,7 +522,8 @@
     )
     chunk = sds((devices, DV + TAIL, lanes), BF16)
     ends = call(ends_kernel, chunk, (2 * 10**9, 3 << 20), keys, values, fwd_decay, bwd_decay)
-    arrived, states = exchange_many(0, outgoing.reshape(devices, capacity, share), ends)
+    (arrived,) = exchange_many(0, outgoing.reshape(devices, capacity, share))
+    states = exchange(ends)
     inbound = gather_parts(arrived.reshape(slots, share))
 
     x = slot_tokens[0]
@@ -504,7 +538,7 @@
         (
             sds((heads, rows, rows), BF16),
             sds((rows, vwidth), F32),
-            sds((rows, vwidth), BF16),
+            sds((devices, rows, vwidth), BF16),
             sds((DV, lanes), F32),
             sds((DV, lanes), F32),
         ),
@@ -517,7 +551,7 @@
         bwd_decay,
     )
 
-    everyone = exchange(jnp.broadcast_to(mixed_rows[None], (devices, rows, vwidth)))
+    everyone = exchange(mixed_rows)
     last = inbound[1], inbound[parts - 1], mixed_rows, gate, upper
     inbound[1], inbound[parts - 1], mixed_rows, gate, upper = lax.optimization_barrier(last)
     act_grad = 0.0
@@ -553,7 +587,7 @@
     streams = gather_parts(stream)
     do, cots, columns = call(
         functools.partial(cotangent_kernel, parts=parts),
-        (sds((rows, vwidth), BF16), chunk, sds((devices, rows, width // devices), BF16)),
+        (sds((rows, vwidth), BF16), chunk, sds((devices, rows // parts, width // devices), BF16)),
         (2 * 10**9, 4 << 20),
         *streams,
         out_proj,
@@ -588,7 +622,12 @@
             pltpu.VMEM(columns.shape, BF16),
             pltpu.VMEM((rows, vwidth), F32),
         ]
-        + sems(devices, 2),
+        + sems(devices, 2)
+        + [
+            pltpu.VMEM((parts,) + columns.shape, BF16),
+            pltpu.SemaphoreType.DMA((parts - 1,)),
+            pltpu.SemaphoreType.DMA((parts - 1,)),
+        ],
         compiler_params=send_params(2),
     )
     return (grad_gate[None], grad_up[None], grad_down[None], proj_grad, dq, dk, dv)

time: 155 us -> 148 us (0.955)
  the two profiles are of different devices: /device:TPU:14 before, /device:TPU:0 now
where the time goes in v3:
time: 148 us; the launch traced here: 147 us
  Pallas kernels  82.5 us (56%)
  matrix products  19.7 us (13%)
  waiting for transfers between devices  16.2 us (11%)
  starting transfers between devices  15.9 us (11%)
  local copies, waits for them, and re-layouts  11.4 us (8%)
    pallas_call x8, Pallas kernels, call(): pl.pallas_call(kernel, out_shape=outs, in_specs=[pl.BlockSpec(memory_spac...  77.2 us
    dot_general x13, matrix products, mm(): lax.dot_general(a, b, ((contract[:1], contract[1:]), ((), ())), preferred...  14.7 us
    ppermute x9, waiting for transfers between devices, swap(): return lax.ppermute(array, 'tp', [(i, i ^ bit) for i in range(parts)])  12.6 us
    all_to_all x2, starting transfers between devices, exchange(): return lax.all_to_all(array, 'sp', split_axis=0, concat_axis=0, tiled=True)  12.4 us
    unnamed x42, local copies, waits for them, and re-layouts  11.4 us
    pallas_call x1, Pallas kernels, weight_grads(): pl.pallas_call(weight_kernel, out_shape=(out, out), grid=(width // tile,)...  5.27 us
    all_to_all x2, waiting for transfers between devices, exchange(): return lax.all_to_all(array, 'sp', split_axis=0, concat_axis=0, tiled=True)  3.67 us
    ppermute x9, starting transfers between devices, swap(): return lax.ppermute(array, 'tp', [(i, i ^ bit) for i in range(parts)])  3.46 us
  transfers between devices with their start and end apart: 11, of which 4 were waited for; matrix products, arithmetic and copies ran while one was open for 13% of the time, Pallas kernels for 23%

profile of v3, /device:TPU:0, one launch (start us, length us, event | category | flops | bytes accessed | tf_op | source)
XLA Modules:
  0.0 146.6 jit_solution(17008951262195653828)
XLA Ops:
  0.6 0.0 copy-start
  0.6 1.5 %copy.20.routes_ref = s32[192,2]{1,0:T(8,128)} copy(s32[192,2]{0,1:T(2,128)} %param.14) | data formatting | bytes 3072 | tf_op args[1]
  2.2 1.4 copy.21.weight_ref
  3.6 3.1 %shard_map.180 = (bf16[576,512]{1,0:T(8,128)(2,1)}, bf16[192,576]{1,0:T(8,128)(2,1)}, bf16[192,512]{1,0:T(8,128)(2,1)}) custom-call(s32[192,2]{1,0:T(8,128)} %copy.20.routes_ref, f32[192,2]{1,0:T(8,128)} %copy.21.weight_ref, bf16[192,2048]{1,0:T(8,128)(2,1)} %grad_ref.1), custom_call_target="tpu_custom_call" | custom-call | flops 452984832 | bytes 3145728 | tf_op jit(solution)/shard_map/pallas_call | solution.py:33
  6.7 17.5 %shard_map.181 = bf16[8,72,512]{2,1,0:T(8,128)(2,1)} custom-call(bf16[8,72,512]{2,1,0:T(8,128)(2,1)} %bitcast.84), custom_call_target="tpu_custom_call" | custom-call | flops 2000000000 | bytes 8388608 | tf_op jit(solution)/shard_map/pallas_call | solution.py:33
  24.2 1.6 %collective-permute-start.1 = (bf16[576,512]{1,0:T(8,128)(2,1)}, bf16[576,512]{1,0:T(8,128)(2,1)}, u32[]{:S(2)}, u32[]{:S(2)}) collective-permute-start(bf16[576,512]{1,0:T(8,128)(2,1)} %bitcast.74), channel_id=1, source_target_pairs={{0,2},{1,3},{2,0},{3,1},{4,6},{5,7},{6,4},{7,5},{8,10},{9,11},{10,... | collective-permute-start | bytes 1769480 | tf_op jit(solution)/shard_map/ppermute | solution.py:504
  25.8 2.5 %shard_map.182 = bf16[8,144,128]{2,1,0:T(8,128)(2,1)} custom-call(bf16[192,128]{1,0:T(8,128)(2,1)} %k_ref.5, bf16[192,256]{1,0:T(8,128)(2,1)} %v_ref.5, f32[192,128]{1,0:T(8,128)} %fwd_ref.5, f32[192,128]{1,0:T(8,128)} %bwd_ref.5), custom_call_target="tpu_custom_call" | custom-call | flops 2000000000 | bytes 3145728 | tf_op jit(solution)/shard_map/pallas_call | solution.py:33
  28.3 8.7 %all-to-all-start = ((bf16[8,144,128]{2,1,0:T(8,128)(2,1)}), bf16[8,144,128]{2,1,0:T(8,128)(2,1)S(1)}, u32[]{:S(2)}, u32[]{:S(2)}) async-start(bf16[8,144,128]{2,1,0:T(8,128)(2,1)} %shard_map.182), calls=%async_computation | async-start | bytes 589824 | tf_op jit(solution)/shard_map/all_to_all | solution.py:473
  37.0 0.0 copy-start.4
  37.0 0.0 copy-start.12
  37.0 3.4 %fusion.9 = f32[576,256]{1,0:T(8,128)} fusion(bf16[1,2048,256]{2,1,0:T(8,128)(2,1)S(1)} %copy-done, bf16[1,576,2048]{2,1,0:T(8,128)(2,1)} %param.16), kind=kOutput, calls=%fused_computation.20 | convolution fusion | flops 603979776 | bytes 3997696 | tf_op jit(solution)/shard_map/dot_general | solution.py:531
  40.4 1.6 %fusion.7 = f32[576,256]{1,0:T(8,128)} fusion(bf16[1,2048,256]{2,1,0:T(8,128)(2,1)S(1)} %copy-done.4, bf16[1,576,2048]{2,1,0:T(8,128)(2,1)S(1)} %copy-done.12), kind=kOutput, calls=%fused_computation.18 | convolution fusion | flops 603979776 | bytes 3997696 | tf_op jit(solution)/shard_map/dot_general | solution.py:532
  42.0 0.2 collective-permute-start.2
  42.2 1.3 fusion.30
  43.5 3.7 %all-to-all-done.in_ref = bf16[8,144,128]{2,1,0:T(8,128)(2,1)S(1)} async-done(((bf16[8,144,128]{2,1,0:T(8,128)(2,1)}), bf16[8,144,128]{2,1,0:T(8,128)(2,1)S(1)}, u32[]{:S(2)}, u32[]{:S(2)}) %all-to-all-start) | async-done | bytes 294944 | tf_op jit(solution)/shard_map/all_to_all | solution.py:473
  47.2 0.7 copy-done.8
  47.9 3.7 %shard_map.183 = (bf16[2,192,192]{2,1,0:T(8,128)(2,1)}, f32[192,256]{1,0:T(8,128)}, bf16[8,192,256]{2,1,0:T(8,128)(2,1)}, f32[128,128]{1,0:T(8,128)}, f32[128,128]{1,0:T(8,128)}) custom-call(bf16[8,144,128]{2,1,0:T(8,128)(2,1)} %copy-done.8, bf16[192,128]{1,0:T(8,128)(2,1)} %q_ref.3, bf16[192,128]{1,0:T(8,128)(2,1)} %k_ref.5, bf16[192,256]{1,0:T(8,128)(2,1)} %v_ref.5, ...), custom_call_target="tpu_custom_call" | custom-call | flops 4000000000 | bytes 3145728 | tf_op jit(solution)/shard_map/pallas_call | solution.py:33
  51.6 3.7 %all-to-all-start.1 = ((bf16[8,192,256]{2,1,0:T(8,128)(2,1)}), bf16[8,192,256]{2,1,0:T(8,128)(2,1)S(1)}, u32[]{:S(2)}, u32[]{:S(2)}) async-start(bf16[8,192,256]{2,1,0:T(8,128)(2,1)} %get-tuple-element.33), calls=%async_computation.1 | async-start | bytes 1572864 | tf_op jit(solution)/shard_map/all_to_all | solution.py:473
  55.4 1.6 %convolution_add_fusion.6 = f32[576,256]{1,0:T(8,128)S(1)} fusion(f32[576,256]{1,0:T(8,128)S(1)} %fusion.30, bf16[576,512]{1,0:T(8,128)(2,1)} %collective-permute-done.refs_1_, bf16[1,256,2048]{2,1,0:T(8,128)(2,1)} %param.19, s32[]{:T(128)S(6)} %select_n.9), kind=kOutput, calls=%fused_computation.12 | convolution fusion | flops 151142400 | bytes 2031620 | tf_op jit(solution)/shard_map/dot_general | solution.py:22
  57.0 1.5 %convolution_add_fusion.5 = f32[576,256]{1,0:T(8,128)S(1)} fusion(f32[576,256]{1,0:T(8,128)S(1)} %convolution_add_fusion.6, bf16[576,512]{1,0:T(8,128)(2,1)} %collective-permute-done.1.refs_2_, bf16[1,256,2048]{2,1,0:T(8,128)(2,1)S(1)} %copy-done.6, s32[]{:T(128)S(6)} %select_n.10), kind=kOutput, calls=%fused_computation.11 | convolution fusion | flops 151142400 | bytes 2031620 | tf_op jit(solution)/shard_map/dot_general | solution.py:22
  58.5 2.3 %multiply_convert_fusion.1 = (bf16[576,256]{1,0:T(8,128)(2,1)S(1)}, bf16[576,256]{1,0:T(8,128)(2,1)S(1)}, bf16[576,256]{1,0:T(8,128)(2,1)}) fusion(f32[576,256]{1,0:T(8,128)S(1)} %copy-done.16, f32[576,256]{1,0:T(8,128)S(1)} %copy-done.17, f32[576,256]{1,0:T(8,128)S(1)} %convolution_add_fusion.5, bf16[576,512]{1,0:T(8,128)(2,1)} %collective-permute-done.2.refs_3_, ...), kind=kOutput, calls=%fused_computation.23 | convolution fusion | flops 153501696 | bytes 3506180 | tf_op jit(solution)/shard_map/dot_general | solution.py:22
  60.8 0.3 fusion.20
  61.2 0.3 fusion.2
  61.5 0.1 collective-permute-start.3
  61.6 0.4 fusion.12
  62.0 1.2 fusion.5
  63.1 0.5 collective-permute-start.5
  63.6 0.3 fusion.25
  64.0 1.2 add_convert_fusion.2
  65.2 0.5 collective-permute-start.4
  65.7 0.3 fusion.17
  66.1 5.3 %shard_map.184 = (bf16[2048,256]{1,0:T(8,128)(2,1)}, bf16[2048,256]{1,0:T(8,128)(2,1)}) custom-call(bf16[576,2048]{1,0:T(8,128)(2,1)} %bitcast.80, bf16[576,256]{1,0:T(8,128)(2,1)} %copy-done.3, bf16[576,256]{1,0:T(8,128)(2,1)} %copy-done.1), custom_call_target="tpu_custom_call" | custom-call | flops 3000000000 | bytes 5242880 | tf_op jit(solution)/shard_map/pallas_call | solution.py:330
  71.3 3.7 %shard_map.185 = bf16[256,2048]{1,0:T(8,128)(2,1)} custom-call(bf16[576,256]{1,0:T(8,128)(2,1)} %get-tuple-element.59.act_ref, bf16[576,512]{1,0:T(8,128)(2,1)} %bitcast.76, bf16[576,512]{1,0:T(8,128)(2,1)} %collective-permute-done.refs_1_, bf16[576,512]{1,0:T(8,128)(2,1)} %collective-permute-done.1.refs_2_, bf16[576,512]{1,0:T(8,128)(2,1)} %collective-permute-done.2.refs_3_), custom_call_target="tpu_custom_call" | custom-call | flops 2000000000 | bytes 4194304 | tf_op jit(solution)/shard_map/pallas_call | solution.py:33
  75.1 5.7 %collective-permute-done.4 = bf16[576,512]{1,0:T(8,128)(2,1)} collective-permute-done((bf16[576,512]{1,0:T(8,128)(2,1)}, bf16[576,512]{1,0:T(8,128)(2,1)}, u32[]{:S(2)}, u32[]{:S(2)}) %collective-permute-start.4) | collective-permute-done | bytes 589856 | tf_op jit(solution)/shard_map/ppermute | solution.py:504
  80.8 2.5 %add_convert_fusion = bf16[576,512]{1,0:T(8,128)(2,1)} fusion(bf16[576,512]{1,0:T(8,128)(2,1)} %collective-permute-done.4, bf16[576,512]{1,0:T(8,128)(2,1)} %collective-permute-done.5, f32[576,512]{1,0:T(8,128)S(1)} %fusion.17, bf16[576,256]{1,0:T(8,128)(2,1)S(1)} %copy-done.2, bf16[1,2048,256]{2,1,0:T(8,128)(2,1)} %param.18, s32[]{:T(128)S(6)} %select_n.8), kind=kOutput, calls=%fused_computation.14 | convolution fusion | flops 153944064 | bytes 3506180 | tf_op jit(solution)/shard_map/dot_general | solution.py:22
  83.3 15.4 %shard_map.186 = bf16[8,72,512]{2,1,0:T(8,128)(2,1)} custom-call(bf16[8,72,512]{2,1,0:T(8,128)(2,1)} %bitcast.79), custom_call_target="tpu_custom_call" | custom-call | flops 2000000000 | bytes 8388608 | tf_op jit(solution)/shard_map/pallas_call | solution.py:33
  98.8 1.4 fusion.6.refs_0_
  100.2 0.6 collective-permute-start.7
  100.8 5.4 %collective-permute-done.7.refs_2_ = bf16[192,512]{1,0:T(8,128)(2,1)S(1)} collective-permute-done((bf16[192,512]{1,0:T(8,128)(2,1)S(1)}, bf16[192,512]{1,0:T(8,128)(2,1)S(1)}, u32[]{:S(2)}, u32[]{:S(2)}) %collective-permute-start.7) | collective-permute-done | bytes 196640 | tf_op jit(solution)/shard_map/ppermute | solution.py:504
  106.2 1.4 collective-permute-done.8.refs_3_
  107.7 0.7 copy-done.15
  108.3 3.5 %shard_map.187 = (bf16[192,256]{1,0:T(8,128)(2,1)}, bf16[8,144,128]{2,1,0:T(8,128)(2,1)}, bf16[8,48,256]{2,1,0:T(8,128)(2,1)}) custom-call(bf16[192,512]{1,0:T(8,128)(2,1)} %copy-done.11, bf16[192,512]{1,0:T(8,128)(2,1)} %copy-done.14, bf16[192,512]{1,0:T(8,128)(2,1)} %copy-done.13, bf16[192,512]{1,0:T(8,128)(2,1)} %copy-done.15, bf16[2048,256]{1,0:T(8,128)(2,1)} %refs_4_.1, ...), custom_call_target="tpu_custom_call" | custom-call | flops 2000000000 | bytes 4194304 | tf_op jit(solution)/shard_map/pallas_call | solution.py:33
  111.8 0.9 copy-done.5
  112.7 27.8 %shard_map.188 = (bf16[192,128]{1,0:T(8,128)(2,1)}, bf16[192,128]{1,0:T(8,128)(2,1)}, bf16[192,256]{1,0:T(8,128)(2,1)}, f32[256,256]{1,0:T(8,128)}) custom-call(bf16[8,144,128]{2,1,0:T(8,128)(2,1)} %get-tuple-element.47.cot_ref, bf16[8,48,256]{2,1,0:T(8,128)(2,1)} %get-tuple-element.48.column_ref, bf16[8,192,256]{2,1,0:T(8,128)(2,1)} %copy-done.5, ...), custom_call_target="tpu_custom_call" | custom-call | flops 4000000000 | bytes 8388608 | tf_op jit(solution)/shard_map/pallas_call | solution.py:33
  140.5 1.7 %copy.26 = f32[256,256]{1,0:T(8,128)} copy(f32[256,256]{1,0:T(8,128)} %get-tuple-element.70) | data formatting | bytes 524288
  142.2 1.4 copy.27
  143.6 1.4 copy.28
  145.0 1.5 %copy.29 = bf16[192,256]{1,0:T(8,128)(2,1)} copy(bf16[192,256]{1,0:T(8,128)(2,1)} %get-tuple-element.73) | data formatting | bytes 196608
  (40 shorter events, 0.1 us)
Async XLA Ops:
  0.6 36.3 %copy-start = (bf16[1,2048,256]{2,1,0:T(8,128)(2,1)S(1)}, bf16[1,2048,256]{2,1,0:T(8,128)(2,1)}, u32[]{:S(2)}) copy-start(bf16[1,2048,256]{2,1,0:T(8,128)(2,1)} %param.17) | copy-start | bytes 3145732
  24.2 17.8 %collective-permute-start.1 = (bf16[576,512]{1,0:T(8,128)(2,1)}, bf16[576,512]{1,0:T(8,128)(2,1)}, u32[]{:S(2)}, u32[]{:S(2)}) collective-permute-start(bf16[576,512]{1,0:T(8,128)(2,1)} %bitcast.74), channel_id=1, source_target_pairs={{0,2},{1,3},{2,0},{3,1},{4,6},{5,7},{6,4},{7,5},{8,10},{9,11},{10,... | collective-permute-start | bytes 1769480 | tf_op jit(solution)/shard_map/ppermute | solution.py:504
  25.8 29.6 %collective-permute-start = (bf16[576,512]{1,0:T(8,128)(2,1)}, bf16[576,512]{1,0:T(8,128)(2,1)}, u32[]{:S(2)}, u32[]{:S(2)}) collective-permute-start(bf16[576,512]{1,0:T(8,128)(2,1)} %bitcast.75), channel_id=1, source_target_pairs={{0,1},{1,0},{2,3},{3,2},{4,5},{5,4},{6,7},{7,6},{8,9},{9,8},{10,11... | collective-permute-start | bytes 1769480 | tf_op jit(solution)/shard_map/ppermute | solution.py:504
  28.3 18.9 %all-to-all-start = ((bf16[8,144,128]{2,1,0:T(8,128)(2,1)}), bf16[8,144,128]{2,1,0:T(8,128)(2,1)S(1)}, u32[]{:S(2)}, u32[]{:S(2)}) async-start(bf16[8,144,128]{2,1,0:T(8,128)(2,1)} %shard_map.182), calls=%async_computation | async-start | bytes 589824 | tf_op jit(solution)/shard_map/all_to_all | solution.py:473
  37.0 3.4 %copy-start.4 = (bf16[1,2048,256]{2,1,0:T(8,128)(2,1)S(1)}, bf16[1,2048,256]{2,1,0:T(8,128)(2,1)}, u32[]{:S(2)}) copy-start(bf16[1,2048,256]{2,1,0:T(8,128)(2,1)} %param.18) | copy-start | bytes 3145732
  37.0 3.4 %copy-start.12 = (bf16[1,576,2048]{2,1,0:T(8,128)(2,1)S(1)}, bf16[1,576,2048]{2,1,0:T(8,128)(2,1)}, u32[]{:S(2)}) copy-start(bf16[1,576,2048]{2,1,0:T(8,128)(2,1)} %param.16) | copy-start | bytes 7077892
  40.4 1.8 %copy-start.7 = (bf16[8,72,512]{2,1,0:T(8,128)(2,1)S(1)}, bf16[8,72,512]{2,1,0:T(8,128)(2,1)}, u32[]{:S(2)}) copy-start(bf16[8,72,512]{2,1,0:T(8,128)(2,1)} %shard_map.181) | copy-start | bytes 1769476
  42.0 13.4 %collective-permute-start.2 = (bf16[576,512]{1,0:T(8,128)(2,1)}, bf16[576,512]{1,0:T(8,128)(2,1)}, u32[]{:S(2)}, u32[]{:S(2)}) collective-permute-start(bf16[576,512]{1,0:T(8,128)(2,1)} %collective-permute-done.1.refs_2_), channel_id=1, source_target_pairs={{0,1},{1,0},{2,3},{3,2},{4,5},{5,4},{6,7},{7,6},{8,9},{9,8},{10,11... | collective-permute-start | bytes 1769480 | tf_op jit(solution)/shard_map/ppermute | solution.py:504
  47.2 0.7 copy-start.8
  51.6 60.2 %all-to-all-start.1 = ((bf16[8,192,256]{2,1,0:T(8,128)(2,1)}), bf16[8,192,256]{2,1,0:T(8,128)(2,1)S(1)}, u32[]{:S(2)}, u32[]{:S(2)}) async-start(bf16[8,192,256]{2,1,0:T(8,128)(2,1)} %get-tuple-element.33), calls=%async_computation.1 | async-start | bytes 1572864 | tf_op jit(solution)/shard_map/all_to_all | solution.py:473
  55.4 1.6 %copy-start.6 = (bf16[1,256,2048]{2,1,0:T(8,128)(2,1)S(1)}, bf16[1,256,2048]{2,1,0:T(8,128)(2,1)}, u32[]{:S(2)}) copy-start(bf16[1,256,2048]{2,1,0:T(8,128)(2,1)} %param.19) | copy-start | bytes 3145732
  57.0 1.6 %copy-start.16 = (f32[576,256]{1,0:T(8,128)S(1)}, f32[576,256]{1,0:T(8,128)}, u32[]{:S(2)}) copy-start(f32[576,256]{1,0:T(8,128)} %fusion.9) | copy-start | bytes 1769476
  57.0 1.5 %copy-start.17 = (f32[576,256]{1,0:T(8,128)S(1)}, f32[576,256]{1,0:T(8,128)}, u32[]{:S(2)}) copy-start(f32[576,256]{1,0:T(8,128)} %fusion.7) | copy-start | bytes 1769476
  60.8 3.2 %copy-start.1 = (bf16[576,256]{1,0:T(8,128)(2,1)}, bf16[576,256]{1,0:T(8,128)(2,1)S(1)}, u32[]{:S(2)}) copy-start(bf16[576,256]{1,0:T(8,128)(2,1)S(1)} %get-tuple-element.57.up_ref) | copy-start | bytes 884740
  60.8 4.9 %copy-start.3 = (bf16[576,256]{1,0:T(8,128)(2,1)}, bf16[576,256]{1,0:T(8,128)(2,1)S(1)}, u32[]{:S(2)}) copy-start(bf16[576,256]{1,0:T(8,128)(2,1)S(1)} %get-tuple-element.58.gate_ref) | copy-start | bytes 884740
  61.5 2.4 %collective-permute-start.3 = (bf16[576,512]{1,0:T(8,128)(2,1)S(1)}, bf16[576,512]{1,0:T(8,128)(2,1)S(1)}, u32[]{:S(2)}, u32[]{:S(2)}) collective-permute-start(bf16[576,512]{1,0:T(8,128)(2,1)S(1)} %fusion.2), channel_id=1, source_target_pairs={{0,1},{1,0},{2,3},{3,2},{4,5},{5,4},{6,7},{7,6},{8,9},{9,8},{10,11... | collective-permute-start | bytes 1769480 | tf_op jit(solution)/shard_map/ppermute | solution.py:504
  63.1 17.6 %collective-permute-start.5 = (bf16[576,512]{1,0:T(8,128)(2,1)}, bf16[576,512]{1,0:T(8,128)(2,1)}, u32[]{:S(2)}, u32[]{:S(2)}) collective-permute-start(bf16[576,512]{1,0:T(8,128)(2,1)} %fusion.5), channel_id=1, source_target_pairs={{0,1},{1,0},{2,3},{3,2},{4,5},{5,4},{6,7},{7,6},{8,9},{9,8},{10,11... | collective-permute-start | bytes 1769480 | tf_op jit(solution)/shard_map/ppermute | solution.py:504
  65.2 15.6 %collective-permute-start.4 = (bf16[576,512]{1,0:T(8,128)(2,1)}, bf16[576,512]{1,0:T(8,128)(2,1)}, u32[]{:S(2)}, u32[]{:S(2)}) collective-permute-start(bf16[576,512]{1,0:T(8,128)(2,1)} %add_convert_fusion.2), channel_id=1, source_target_pairs={{0,2},{1,3},{2,0},{3,1},{4,6},{5,7},{6,4},{7,5},{8,10},{9,11},{10,... | collective-permute-start | bytes 1769480 | tf_op jit(solution)/shard_map/ppermute | solution.py:504
  71.3 9.4 %copy-start.2 = (bf16[576,256]{1,0:T(8,128)(2,1)S(1)}, bf16[576,256]{1,0:T(8,128)(2,1)}, u32[]{:S(2)}) copy-start(bf16[576,256]{1,0:T(8,128)(2,1)} %copy-done.1) | copy-start | bytes 884740
  83.3 15.5 %copy-start.9 = (bf16[192,576]{1,0:T(8,128)(2,1)S(1)}, bf16[192,576]{1,0:T(8,128)(2,1)}, u32[]{:S(2)}) copy-start(bf16[192,576]{1,0:T(8,128)(2,1)} %get-tuple-element.44) | copy-start | bytes 663556
  83.3 15.5 %copy-start.10 = (bf16[192,512]{1,0:T(8,128)(2,1)S(1)}, bf16[192,512]{1,0:T(8,128)(2,1)}, u32[]{:S(2)}) copy-start(bf16[192,512]{1,0:T(8,128)(2,1)} %get-tuple-element.43) | copy-start | bytes 589828
  100.2 7.5 %copy-start.11 = (bf16[192,512]{1,0:T(8,128)(2,1)}, bf16[192,512]{1,0:T(8,128)(2,1)S(1)}, u32[]{:S(2)}) copy-start(bf16[192,512]{1,0:T(8,128)(2,1)S(1)} %fusion.6.refs_0_) | copy-start | bytes 589828
  100.2 6.0 %collective-permute-start.7 = (bf16[192,512]{1,0:T(8,128)(2,1)S(1)}, bf16[192,512]{1,0:T(8,128)(2,1)S(1)}, u32[]{:S(2)}, u32[]{:S(2)}) collective-permute-start(bf16[192,512]{1,0:T(8,128)(2,1)S(1)} %fusion.6.refs_0_), channel_id=1, source_target_pairs={{0,2},{1,3},{2,0},{3,1},{4,6},{5,7},{6,4},{7,5},{8,10},{9,11},{10,... | collective-permute-start | bytes 589832 | tf_op jit(solution)/shard_map/ppermute | solution.py:504
  100.8 5.4 %collective-permute-start.6 = (bf16[192,512]{1,0:T(8,128)(2,1)S(1)}, bf16[192,512]{1,0:T(8,128)(2,1)S(1)}, u32[]{:S(2)}, u32[]{:S(2)}) collective-permute-start(bf16[192,512]{1,0:T(8,128)(2,1)S(1)} %fusion.6.refs_0_), channel_id=1, source_target_pairs={{0,1},{1,0},{2,3},{3,2},{4,5},{5,4},{6,7},{7,6},{8,9},{9,8},{10,11... | collective-permute-start | bytes 589832 | tf_op jit(solution)/shard_map/ppermute | solution.py:504
  106.2 1.5 copy-start.13
  106.2 1.4 collective-permute-start.8
  106.2 1.4 copy-start.14
  107.7 0.7 copy-start.15
  111.8 0.9 copy-start.5
